TPU v7x, 128 devices: a whole 4x4x4 slice. The times are simulated.
128 devices in a mesh: ep: 16 (over z, x), tp: 8 (over y, core).
Axes of the slice: x: 4, y: 4, z: 4, core: 2. Of those that a mesh axis runs over, the one named last changes fastest.
Arguments:
- tokens: bfloat16 [4096, 2048], P('ep'), may hold values from -40 to 40
- cotangent: bfloat16 [4096, 2048], P('ep'), may hold values from -6 to 6
- expert_ids: int32 [4096, 4], P('ep'), may hold values from 0 to 31, all different within a row; in each aligned block of 256 rows (0 to 255, 256 to 511, ...) at most 48 rows name the same one
- route_weights: bfloat16 [4096, 4], P('ep'), may hold values from 0.099609375 to 1
- gate_weight: bfloat16 [32, 2048, 2048], P('ep', None, 'tp'), may hold values from -0.125 to 0.125
- up_weight: bfloat16 [32, 2048, 2048], P('ep', None, 'tp'), may hold values from -0.125 to 0.125
- down_weight: bfloat16 [32, 2048, 2048], P('ep', 'tp'), may hold values from -0.125 to 0.125
- dense_weight: bfloat16 [2048, 2048], P('tp', 'ep'), may hold values from -0.125 to 0.125
- dense_gate: float32 [2048], replicated, may hold values from 0.1 to 1.9
Outputs:
- token_grad: bfloat16 [4096, 2048], P('ep', 'tp')
- weight_grad: bfloat16 [4096, 4], P('ep')
- gate_grad: float32 [32, 2048, 2048], P('ep', None, 'tp')
- up_grad: float32 [32, 2048, 2048], P('ep', None, 'tp')
- down_grad: float32 [32, 2048, 2048], P('ep', 'tp')
- dense_grad: float32 [2048, 2048], P('tp', 'ep')
Inputs may be any that keep to these rules, and one draw needn't show every extreme that they name: `expert_ids`: in the rows of one device, at most 48 routed rows name any one expert, and in every draw some expert is named by exactly 48 rows of some device.
All inputs are finite; a program needn't handle non-finite values.
Results may differ from a plain program's by a relative error of at most 0.02.
Values may be sent and summed in bfloat16 or wider, within the bound.
A program may use at most 128 MiB of HBM per device.

v0:
```python
import jax
import jax.numpy as jnp
from jax import lax
from jax.sharding import PartitionSpec as P

clamp_limit = 7.0
sigmoid_slope = 1.702


def side_by_side(arrays, axis, dim, along):
    both = jnp.concatenate(arrays, axis=along)
    filled, at, done = (lax.all_gather(both, axis, axis=dim, tiled=True), 0, [])
    for a in arrays:
        done.append(lax.slice_in_dim(filled, at, at + a.shape[along], axis=along))
        at += a.shape[along]
    return tuple(done)


def from_everyone(array, axis):
    copies = jnp.broadcast_to(array, (lax.axis_size(axis), *array.shape))
    return lax.all_to_all(copies, axis, split_axis=0, concat_axis=0, tiled=True)


def joined_along(tiles, dim):
    lengths = list(tiles.shape[1:])
    lengths[dim] *= tiles.shape[0]
    return jnp.moveaxis(tiles, 0, dim).reshape(lengths)


def gather_directly(array, axis, dim):
    tiles = from_everyone(array, axis)
    return joined_along(tiles, dim)


def cut_along(array, dim, peers):
    lengths = array.shape
    tiles = array.reshape(*lengths[:dim], peers, lengths[dim] // peers, *lengths[dim + 1 :])
    return jnp.moveaxis(tiles, dim, 0)


def summed_on_arrival(array, axis, dim):
    peers = lax.axis_size(axis)
    tiles = lax.all_to_all(cut_along(array, dim, peers), axis, 0, 0, tiled=True)
    return jnp.sum(tiles.astype(jnp.float32), axis=0)


def expert_back(row_input, row_cotan, row_weight, w_gate, w_up, w_down):
    gate_pre = jnp.dot(row_input, w_gate, preferred_element_type=jnp.float32)
    up_pre = jnp.dot(row_input, w_up, preferred_element_type=jnp.float32)
    gate_val = jnp.minimum(gate_pre, clamp_limit)
    up_val = jnp.clip(up_pre, -clamp_limit, clamp_limit)
    squash = jax.nn.sigmoid(sigmoid_slope * gate_val)
    hidden = ((up_val + 1.0) * gate_val * squash).astype(jnp.bfloat16)
    down_back = lax.dot_general(
        row_cotan, w_down, (((1,), (1,)), ((), ())), preferred_element_type=jnp.float32
    )
    scores = jnp.sum(hidden.astype(jnp.float32) * down_back, axis=1)
    scale_col = row_weight.astype(jnp.float32)[:, None]
    hidden_back = scale_col * down_back
    gate_slope = squash + sigmoid_slope * gate_val * squash * (1.0 - squash)
    gate_back = jnp.where(
        gate_pre < clamp_limit, hidden_back * (up_val + 1.0) * gate_slope, 0.0
    ).astype(jnp.bfloat16)
    up_back = jnp.where(jnp.abs(up_pre) < clamp_limit, hidden_back * gate_val * squash, 0.0).astype(
        jnp.bfloat16
    )
    weighted = (scale_col * row_cotan.astype(jnp.float32)).astype(jnp.bfloat16)
    input_back = lax.dot_general(
        gate_back, w_gate, (((1,), (1,)), ((), ())), preferred_element_type=jnp.float32
    )
    input_back = input_back + lax.dot_general(
        up_back, w_up, (((1,), (1,)), ((), ())), preferred_element_type=jnp.float32
    )
    grad_gate = lax.dot_general(
        row_input, gate_back, (((0,), (0,)), ((), ())), preferred_element_type=jnp.float32
    )
    grad_up = lax.dot_general(
        row_input, up_back, (((0,), (0,)), ((), ())), preferred_element_type=jnp.float32
    )
    grad_down = lax.dot_general(
        hidden, weighted, (((0,), (0,)), ((), ())), preferred_element_type=jnp.float32
    )
    return (input_back, scores, grad_gate, grad_up, grad_down)


def shards(
    tokens,
    cotangent,
    expert_ids,
    route_weights,
    gate_weight,
    up_weight,
    down_weight,
    dense_weight,
    dense_gate,
):
    tok_rows, model_width = tokens.shape
    top_count = expert_ids.shape[1]
    local_count = gate_weight.shape[0]
    ep_size = lax.axis_size("ep")
    tp_size = lax.axis_size("tp")
    expert_total = local_count * ep_size
    capacity = tok_rows * top_count * 3 // (2 * expert_total)
    routed = tok_rows * top_count
    feature_part = model_width // tp_size
    flat_ids = expert_ids.reshape(routed)
    onehot = (flat_ids[:, None] == jnp.arange(expert_total, dtype=jnp.int32)[None, :]).astype(
        jnp.int32
    )
    row_ranks = jnp.sum(onehot * (jnp.cumsum(onehot, axis=0) - 1), axis=1)
    slot_ids = flat_ids * capacity + row_ranks
    slot_rows = (
        jnp.full((expert_total * capacity,), routed, jnp.int32)
        .at[slot_ids]
        .set(jnp.arange(routed, dtype=jnp.int32))
    )
    slot_tokens = slot_rows // top_count
    zero_row = jnp.zeros((1, model_width), jnp.bfloat16)
    send_input = jnp.concatenate([tokens, zero_row], axis=0)[slot_tokens].reshape(
        ep_size, local_count * capacity, model_width
    )
    send_cotan = jnp.concatenate([cotangent, zero_row], axis=0)[slot_tokens].reshape(
        ep_size, local_count * capacity, model_width
    )
    send_weight = jnp.concatenate([route_weights.reshape(routed), jnp.zeros((1,), jnp.bfloat16)])[
        slot_rows
    ]
    send_weight = send_weight.reshape(ep_size, local_count * capacity)
    feature_start = lax.axis_index("tp") * feature_part
    cut_input = lax.dynamic_slice_in_dim(send_input, feature_start, feature_part, 2)
    cut_cotan = lax.dynamic_slice_in_dim(send_cotan, feature_start, feature_part, 2)
    part_input, part_cotan, recv_weight = (
        lax.all_to_all(cut_input, "ep", split_axis=0, concat_axis=0, tiled=True),
        lax.all_to_all(cut_cotan, "ep", split_axis=0, concat_axis=0, tiled=True),
        lax.all_to_all(send_weight, "ep", split_axis=0, concat_axis=0, tiled=True),
    )
    recv_input, recv_cotan = side_by_side((part_input, part_cotan), "tp", 2, 0)
    input_backs, score_list, gate_list, up_list, down_list = ([], [], [], [], [])
    for local_index in range(local_count):
        low = local_index * capacity
        row_input = recv_input[:, low : low + capacity].reshape(ep_size * capacity, model_width)
        row_cotan = recv_cotan[:, low : low + capacity].reshape(ep_size * capacity, model_width)
        row_weight = recv_weight[:, low : low + capacity].reshape(ep_size * capacity)
        pieces_out = expert_back(
            row_input,
            row_cotan,
            row_weight,
            gate_weight[local_index],
            up_weight[local_index],
            down_weight[local_index],
        )
        input_backs.append(pieces_out[0])
        score_list.append(pieces_out[1])
        gate_list.append(pieces_out[2])
        up_list.append(pieces_out[3])
        down_list.append(pieces_out[4])
    back_terms = jnp.stack(input_backs)
    score_cols = jnp.broadcast_to(
        jnp.stack(score_list)[:, :, None], (local_count, ep_size * capacity, tp_size)
    )
    summed, score_sum = (
        lax.psum_scatter(
            back_terms.astype(jnp.bfloat16), "tp", scatter_dimension=2, tiled=True
        ).astype(jnp.float32),
        lax.psum_scatter(
            score_cols.astype(jnp.bfloat16), "tp", scatter_dimension=2, tiled=True
        ).astype(jnp.float32),
    )
    back_rows = summed.astype(jnp.bfloat16).reshape(local_count, ep_size, capacity, feature_part)
    back_rows = back_rows.transpose(1, 0, 2, 3).reshape(
        ep_size, local_count * capacity, feature_part
    )
    back_score = score_sum[:, :, 0].astype(jnp.bfloat16).reshape(local_count, ep_size, capacity)
    back_score = back_score.transpose(1, 0, 2).reshape(ep_size, local_count * capacity)
    got_rows, got_score = (
        lax.all_to_all(back_rows, "ep", split_axis=0, concat_axis=0, tiled=True),
        lax.all_to_all(back_score, "ep", split_axis=0, concat_axis=0, tiled=True),
    )
    row_back = got_rows.reshape(expert_total * capacity, feature_part)[slot_ids]
    score_rows = got_score.reshape(expert_total * capacity)[slot_ids]
    gated_cotan = (dense_gate[None, :] * cotangent.astype(jnp.float32)).astype(jnp.bfloat16)
    columns = gated_cotan
    dense_back = lax.dot_general(
        columns,
        gather_directly(dense_weight, "ep", 1),
        (((1,), (1,)), ((), ())),
        preferred_element_type=jnp.float32,
    )
    own_input = lax.dynamic_slice_in_dim(
        tokens, lax.axis_index("tp") * feature_part, feature_part, 1
    )
    columns = gated_cotan
    dense_share = summed_on_arrival(
        lax.dot_general(
            columns, own_input, (((0,), (0,)), ((), ())), preferred_element_type=jnp.float32
        ).astype(jnp.bfloat16),
        "ep",
        0,
    )
    dense_grad = dense_share.T
    token_grad = (
        jnp.sum(row_back.reshape(tok_rows, top_count, feature_part).astype(jnp.float32), axis=1)
        + dense_back
    ).astype(jnp.bfloat16)
    weight_grad = score_rows.reshape(tok_rows, top_count)
    return (
        token_grad,
        weight_grad,
        jnp.stack(gate_list),
        jnp.stack(up_list),
        jnp.stack(down_list),
        dense_grad,
    )


def solution(mesh):
    in_specs = (
        P("ep", None),
        P("ep", None),
        P("ep", None),
        P("ep", None),
        P("ep", None, "tp"),
        P("ep", None, "tp"),
        P("ep", "tp", None),
        P("tp", "ep"),
        P(),
    )
    out_specs = (
        P("ep", "tp"),
        P("ep", None),
        P("ep", None, "tp"),
        P("ep", None, "tp"),
        P("ep", "tp", None),
        P("tp", "ep"),
    )
    return jax.shard_map(shards, mesh=mesh, in_specs=in_specs, out_specs=out_specs, check_vma=False)
```

profile of v0, /device:TPU:1, one launch (start us, length us, event | category | flops | bytes accessed | tf_op | source)
XLA Modules:
  0.0 296.5 jit_solution(7874539225803338914)
XLA Ops:
  8.9 9.0 %reduce-window.6 = s32[32,8,128]{2,1,0:T(8,128)S(1)} reduce-window(s32[32,8,128]{2,1,0:T(8,128)S(1)} %fusion.40, s32[]{:T(128)} %constant.13.clone.1), window={size=1x1x128 pad=0_0x0_0x127_0}, to_apply=%region_0.0 | reduce-window | flops 4161536 | bytes 262148 | tf_op jit(solution)/shard_map/reduce-window
  18.7 4.3 %scatter_custom_fusion = s32[1536]{0:T(1024)S(1)} fusion(s32[1024]{0:T(1024)S(1)} %bitcast.129, s32[1024]{0:T(1024)S(1)} %iota.11, s32[]{:T(128)} %constant.21.clone.1), kind=kCustom, calls=%fused_computation.98 | custom fusion | bytes 6148 | tf_op jit(solution)/shard_map/scatter | solution.py:115
  24.4 7.1 %gather_fusion = bf16[1536,2048]{1,0:T(8,128)(2,1)} fusion(bf16[257,2048]{1,0:T(8,128)(2,1)S(1)} %concatenate.12, s32[2048]{0:T(1024)S(1)} %get-tuple-element.39), kind=kCustom, calls=%fused_computation | custom fusion | bytes 12589056 | tf_op jit(solution)/shard_map/gather | solution.py:119
  33.7 8.4 %all-to-all-start = ((bf16[16,96,256]{2,1,0:T(8,128)(2,1)}), bf16[16,96,256]{2,1,0:T(8,128)(2,1)S(1)}, u32[]{:S(2)}, u32[]{:S(2)}) async-start(bf16[16,96,256]{2,1,0:T(8,128)(2,1)} %constant_dynamic-slice_fusion.1), calls=%async_computation | async-start | bytes 1572864 | tf_op jit(solution)/shard_map/all_to_all | solution.py:133
  42.3 7.1 %gather_fusion.1 = bf16[1536,2048]{1,0:T(8,128)(2,1)} fusion(bf16[257,2048]{1,0:T(8,128)(2,1)S(1)} %concatenate.13, s32[2048]{0:T(1024)S(1)} %get-tuple-element.39), kind=kCustom, calls=%fused_computation.1 | custom fusion | bytes 12589056 | tf_op jit(solution)/shard_map/gather | solution.py:122
  50.5 4.8 %all-to-all-done = bf16[16,96,256]{2,1,0:T(8,128)(2,1)S(1)} async-done(((bf16[16,96,256]{2,1,0:T(8,128)(2,1)}), bf16[16,96,256]{2,1,0:T(8,128)(2,1)S(1)}, u32[]{:S(2)}, u32[]{:S(2)}) %all-to-all-start) | async-done | bytes 786464 | tf_op jit(solution)/shard_map/all_to_all | solution.py:133
  55.3 16.6 %all_to_all.48 = bf16[16,96,256]{2,1,0:T(8,128)(2,1)S(1)} all-to-all(bf16[16,96,256]{2,1,0:T(8,128)(2,1)S(1)} %constant_dynamic-slice_fusion), channel_id=1, replica_groups=mesh['ep'=16,'tp'=8] {'ep'}, dimensions={0} | all-to-all | bytes 1572864 | tf_op jit(solution)/shard_map/all_to_all | solution.py:134
  73.6 9.5 %gather_fusion.2 = bf16[1536]{0:T(1024)(128)(2,1)S(1)} fusion(bf16[1025]{0:T(1024)(128)(2,1)S(1)} %pad_maximum_fusion.5, s32[2048]{0:T(1024)S(1)} %get-tuple-element.38), kind=kCustom, calls=%fused_computation.2 | custom fusion | bytes 12288 | tf_op jit(solution)/shard_map/gather | solution.py:125
  83.1 9.0 %all_to_all.49 = bf16[16,1,96]{2,1,0:T(2,128)(2,1)S(1)} all-to-all(bf16[16,1,96]{2,1,0:T(2,128)(2,1)S(1)} %all_to_all.39), channel_id=1, replica_groups=mesh['ep'=16,'tp'=8] {'ep'}, dimensions={0} | all-to-all | bytes 6144 | tf_op jit(solution)/shard_map/all_to_all | solution.py:135
  92.4 52.1 %all-gather.2.cloned.1.call-done = bf16[32,96,2048]{2,1,0:T(8,128)(2,1)} async-done(((bf16[32,96,256]{2,1,0:T(8,128)(2,1)}), bf16[32,96,2048]{2,1,0:T(8,128)(2,1)}) %all-gather.2.cloned.1.call-update) | async-done | bytes 12582928 | tf_op jit(solution)/shard_map/all_gather | solution.py:12
  144.5 5.6 %fusion.46 = (bf16[16,48,2048]{2,1,0:T(8,128)(2,1)S(1)}, bf16[16,48,2048]{2,1,0:T(8,128)(2,1)S(1)}, bf16[16,48,2048]{2,1,0:T(8,128)(2,1)S(1)}, bf16[16,48,2048]{2,1,0:T(8,128)(2,1)S(1)}) fusion(bf16[32,96,2048]{2,1,0:T(8,128)(2,1)} %all-gather.2.cloned.1.call-done), kind=kLoop, calls=%fused_computation.107 | loop fusion | bytes 25165824 | tf_op jit(solution)/shard_map/slice | solution.py:142
  157.1 2.5 multiply_reduce_fusion.1
  160.6 2.5 multiply_reduce_fusion
  166.4 3.2 %pad_maximum_fusion = bf16[2,768,2048]{2,1,0:T(8,128)(2,1)} fusion(bf16[1,768,2048]{2,1,0:T(8,128)(2,1)S(1)} %fusion.5, bf16[1,768,2048]{2,1,0:T(8,128)(2,1)S(1)} %fusion.4), kind=kLoop, calls=%fused_computation.6 | loop fusion | flops 3145728 | bytes 12582912 | tf_op jit(solution)/shard_map/stack | solution.py:157
  169.6 3.0 %convolution_convert_fusion = bf16[2048,256]{1,0:T(8,128)(2,1)} fusion(bf16[256,2048]{1,0:T(8,128)(2,1)} %param.10, f32[2048]{0:T(1024)} %param.17, bf16[256,2048]{1,0:T(8,128)(2,1)} %param.9, s32[]{:T(128)S(6)} %select_n.45), kind=kOutput, calls=%fused_computation.26 | convolution fusion | flops 270532608 | bytes 2236420 | tf_op jit(solution)/shard_map/dot_general | solution.py:194
  172.7 6.7 %all-to-all-start.6 = ((bf16[16,128,256]{2,1,0:T(8,128)(2,1)}), bf16[16,128,256]{2,1,0:T(8,128)(2,1)}, u32[]{:S(2)}, u32[]{:S(2)}) async-start(bf16[16,128,256]{2,1,0:T(8,128)(2,1)} %bitcast.121), calls=%async_computation.7 | async-start | bytes 2097152 | tf_op jit(solution)/shard_map/all_to_all | solution.py:43
  181.6 14.4 %all-to-all-done.6 = bf16[16,128,256]{2,1,0:T(8,128)(2,1)} async-done(((bf16[16,128,256]{2,1,0:T(8,128)(2,1)}), bf16[16,128,256]{2,1,0:T(8,128)(2,1)}, u32[]{:S(2)}, u32[]{:S(2)}) %all-to-all-start.6) | async-done | bytes 1048608 | tf_op jit(solution)/shard_map/all_to_all | solution.py:43
  200.3 23.5 %all-reduce.2 = bf16[2,768,8]{1,0,2:T(2,128)(2,1)} all-reduce(bf16[2,768,8]{1,0,2:T(2,128)(2,1)} %broadcast_in_dim.39), channel_id=3, replica_groups=mesh['ep'=16,'tp'=8] {'tp'}, use_global_device_ids=true, to_apply=%region_8.9.clone | all-reduce | flops 12288 | bytes 49152
  227.2 4.5 %all-to-all-start.5 = ((bf16[16,1,96]{2,1,0:T(2,128)(2,1)}), bf16[16,1,96]{2,1,0:T(2,128)(2,1)S(1)}, u32[]{:S(2)}, u32[]{:S(2)}) async-start(bf16[16,1,96]{2,1,0:T(2,128)(2,1)} %all_to_all.40), calls=%async_computation.6 | async-start | bytes 16384 | tf_op jit(solution)/shard_map/all_to_all | solution.py:177
  231.7 4.5 %convolution_bitcast_fusion.1 = f32[1,2048,256]{2,1,0:T(8,128)} fusion(bf16[768,2048]{1,0:T(8,128)(2,1)} %bitcast.112, bf16[768,256]{0,1:T(8,128)(2,1)} %copy-done.12), kind=kOutput, calls=%fused_computation.23 | convolution fusion | flops 805306368 | bytes 5636096 | tf_op jit(solution)/shard_map/dot_general | solution.py:77
  236.2 2.5 fusion.7
  238.7 2.4 convolution_bitcast_fusion
  243.2 6.7 %all-to-all-start.3 = ((bf16[16,96,256]{2,1,0:T(8,128)(2,1)}), bf16[16,96,256]{2,1,0:T(8,128)(2,1)}, u32[]{:S(2)}, u32[]{:S(2)}) async-start(bf16[16,96,256]{2,1,0:T(8,128)(2,1)} %bitcast.120), calls=%async_computation.4 | async-start | bytes 1572864 | tf_op jit(solution)/shard_map/all_to_all | solution.py:176
  250.0 4.4 %convolution_bitcast_fusion.3 = f32[1,2048,256]{2,1,0:T(8,128)} fusion(bf16[768,2048]{1,0:T(8,128)(2,1)} %bitcast.113, bf16[768,256]{0,1:T(8,128)(2,1)} %copy-done.8), kind=kOutput, calls=%fused_computation.25 | convolution fusion | flops 805306368 | bytes 5636096 | tf_op jit(solution)/shard_map/dot_general | solution.py:74
  256.0 2.3 pad_maximum_fusion.3
  258.3 2.2 all-to-all-done.3
  262.4 4.5 %all-to-all-start.4 = ((bf16[16,256,128]{1,2,0:T(8,128)(2,1)}), bf16[16,256,128]{1,2,0:T(8,128)(2,1)}, u32[]{:S(2)}, u32[]{:S(2)}) async-start(bf16[16,256,128]{1,2,0:T(8,128)(2,1)} %broadcast_in_dim.38), calls=%async_computation.5 | async-start | bytes 2097152 | tf_op jit(solution)/shard_map/all_to_all | solution.py:21
  269.1 2.3 pad_maximum_fusion.2
  271.6 2.3 pad_maximum_fusion.1
  274.0 6.8 %gather_fusion.4 = bf16[1024]{0:T(1024)(128)(2,1)S(1)} fusion(bf16[1536]{0:T(1024)(128)(2,1)S(1)} %reshape.147, s32[1024]{0:T(1024)S(1)} %broadcast_clamp_fusion), kind=kCustom, calls=%fused_computation.4 | custom fusion | bytes 8192 | tf_op jit(solution)/shard_map/gather | solution.py:180
  281.6 4.8 %gather_fusion.3 = bf16[1024,256]{1,0:T(8,128)(2,1)S(1)} fusion(bf16[1536,256]{1,0:T(8,128)(2,1)} %bitcast.21, s32[1024]{0:T(1024)S(1)} %broadcast_clamp_fusion), kind=kCustom, calls=%fused_computation.3 | custom fusion | bytes 1052672 | tf_op jit(solution)/shard_map/gather | solution.py:179
  287.3 2.3 fusion.8
  (123 shorter events, 40.2 us)
Async XLA Ops:
  31.5 10.6 %copy-start.15 = (bf16[256,2048]{1,0:T(8,128)(2,1)S(1)}, bf16[256,2048]{1,0:T(8,128)(2,1)}, u32[]{:S(2)}) copy-start(bf16[256,2048]{1,0:T(8,128)(2,1)} %param.10) | copy-start | bytes 3145732
  33.7 21.7 %all-to-all-start = ((bf16[16,96,256]{2,1,0:T(8,128)(2,1)}), bf16[16,96,256]{2,1,0:T(8,128)(2,1)S(1)}, u32[]{:S(2)}, u32[]{:S(2)}) async-start(bf16[16,96,256]{2,1,0:T(8,128)(2,1)} %constant_dynamic-slice_fusion.1), calls=%async_computation | async-start | bytes 1572864 | tf_op jit(solution)/shard_map/all_to_all | solution.py:133
  42.1 102.4 %all-gather.2.cloned.1.call-start = ((), (), s32[]{:S(2)}) async-start(), calls=%async_computation.8 | async-start | bytes 14155776 | tf_op jit(solution)/shard_map/all_gather | solution.py:12
  50.5 22.8 %copy-start.21 = (bf16[256,4]{0,1:T(4,128)(2,1)S(1)}, bf16[256,4]{0,1:T(4,128)(2,1)}, u32[]{:S(2)}) copy-start(bf16[256,4]{0,1:T(4,128)(2,1)} %param.12) | copy-start | bytes 6148
  73.2 167.9 %reduce-scatter.2.cloned.1.call-start = ((), (), s32[]{:S(2)}) async-start(), calls=%async_computation.9 | async-start | bytes 7077888 | tf_op jit(solution)/shard_map/reduce_scatter | solution.py:162
  92.3 64.2 %copy-start.19 = (f32[768]{0:T(1024)}, f32[768]{0:T(1024)S(1)}, u32[]{:S(2)}) copy-start(f32[768]{0:T(1024)S(1)} %reshape.150) | copy-start | bytes 9220
  92.4 68.2 %copy-start.17 = (f32[768]{0:T(1024)}, f32[768]{0:T(1024)S(1)}, u32[]{:S(2)}) copy-start(f32[768]{0:T(1024)S(1)} %reshape.151) | copy-start | bytes 9220
  144.5 5.7 %copy-start.11 = (bf16[2,2048,256]{2,1,0:T(8,128)(2,1)S(1)}, bf16[2,2048,256]{2,1,0:T(8,128)(2,1)}, u32[]{:S(2)}) copy-start(bf16[2,2048,256]{2,1,0:T(8,128)(2,1)} %param.14) | copy-start | bytes 6291460
  150.1 4.3 %copy-start = (bf16[16,48,2048]{2,1,0:T(8,128)(2,1)}, bf16[16,48,2048]{2,1,0:T(8,128)(2,1)S(1)}, u32[]{:S(2)}) copy-start(bf16[16,48,2048]{2,1,0:T(8,128)(2,1)S(1)} %get-tuple-element.25) | copy-start | bytes 9437188
  150.1 6.4 %copy-start.6 = (bf16[16,48,2048]{2,1,0:T(8,128)(2,1)}, bf16[16,48,2048]{2,1,0:T(8,128)(2,1)S(1)}, u32[]{:S(2)}) copy-start(bf16[16,48,2048]{2,1,0:T(8,128)(2,1)S(1)} %get-tuple-element.22) | copy-start | bytes 9437188
  150.1 10.5 %copy-start.4 = (bf16[16,48,2048]{2,1,0:T(8,128)(2,1)}, bf16[16,48,2048]{2,1,0:T(8,128)(2,1)S(1)}, u32[]{:S(2)}) copy-start(bf16[16,48,2048]{2,1,0:T(8,128)(2,1)S(1)} %get-tuple-element.23) | copy-start | bytes 9437188
  150.1 3.2 %copy-start.9 = (bf16[2,2048,256]{2,1,0:T(8,128)(2,1)S(1)}, bf16[2,2048,256]{2,1,0:T(8,128)(2,1)}, u32[]{:S(2)}) copy-start(bf16[2,2048,256]{2,1,0:T(8,128)(2,1)} %param.13) | copy-start | bytes 6291460
  155.5 1.6 copy-start.22
  159.6 4.6 %copy-start.12 = (bf16[768,256]{0,1:T(8,128)(2,1)}, bf16[768,256]{0,1:T(8,128)(2,1)S(1)}, u32[]{:S(2)}) copy-start(bf16[768,256]{0,1:T(8,128)(2,1)S(1)} %get-tuple-element.31) | copy-start | bytes 1179652
  163.1 2.1 copy-start.13
  169.6 11.3 %copy-start.24 = (u32[128]{0:T(128)S(1)}, u32[128]{0:T(128)}, u32[]{:S(2)}) copy-start(u32[128]{0:T(128)} %constant.67) | copy-start | bytes 1540
  172.7 23.2 %all-to-all-start.6 = ((bf16[16,128,256]{2,1,0:T(8,128)(2,1)}), bf16[16,128,256]{2,1,0:T(8,128)(2,1)}, u32[]{:S(2)}, u32[]{:S(2)}) async-start(bf16[16,128,256]{2,1,0:T(8,128)(2,1)} %bitcast.121), calls=%async_computation.7 | async-start | bytes 2097152 | tf_op jit(solution)/shard_map/all_to_all | solution.py:43
  227.2 16.1 %all-to-all-start.5 = ((bf16[16,1,96]{2,1,0:T(2,128)(2,1)}), bf16[16,1,96]{2,1,0:T(2,128)(2,1)S(1)}, u32[]{:S(2)}, u32[]{:S(2)}) async-start(bf16[16,1,96]{2,1,0:T(2,128)(2,1)} %all_to_all.40), calls=%async_computation.6 | async-start | bytes 16384 | tf_op jit(solution)/shard_map/all_to_all | solution.py:177
  231.7 4.5 %copy-start.7 = (bf16[16,48,2048]{2,1,0:T(8,128)(2,1)S(1)}, bf16[16,48,2048]{2,1,0:T(8,128)(2,1)}, u32[]{:S(2)}) copy-start(bf16[16,48,2048]{2,1,0:T(8,128)(2,1)} %copy-done.6) | copy-start | bytes 9437188
  231.7 4.5 %copy-start.20 = (f32[768]{0:T(1024)S(1)}, f32[768]{0:T(1024)}, u32[]{:S(2)}) copy-start(f32[768]{0:T(1024)} %copy-done.19) | copy-start | bytes 9220
  231.7 4.5 %copy-start.26 = (bf16[768,256]{0,1:T(8,128)(2,1)S(1)}, bf16[768,256]{0,1:T(8,128)(2,1)}, u32[]{:S(2)}) copy-start(bf16[768,256]{0,1:T(8,128)(2,1)} %get-tuple-element.19) | copy-start | bytes 1179652
  236.2 2.5 copy-start.14
  243.2 17.2 %all-to-all-start.3 = ((bf16[16,96,256]{2,1,0:T(8,128)(2,1)}), bf16[16,96,256]{2,1,0:T(8,128)(2,1)}, u32[]{:S(2)}, u32[]{:S(2)}) async-start(bf16[16,96,256]{2,1,0:T(8,128)(2,1)} %bitcast.120), calls=%async_computation.4 | async-start | bytes 1572864 | tf_op jit(solution)/shard_map/all_to_all | solution.py:176
  249.9 4.5 %copy-start.5 = (bf16[16,48,2048]{2,1,0:T(8,128)(2,1)S(1)}, bf16[16,48,2048]{2,1,0:T(8,128)(2,1)}, u32[]{:S(2)}) copy-start(bf16[16,48,2048]{2,1,0:T(8,128)(2,1)} %copy-done.4) | copy-start | bytes 9437188
  250.0 4.5 %copy-start.18 = (f32[768]{0:T(1024)S(1)}, f32[768]{0:T(1024)}, u32[]{:S(2)}) copy-start(f32[768]{0:T(1024)} %copy-done.17) | copy-start | bytes 9220
  250.0 4.5 %copy-start.25 = (bf16[768,256]{0,1:T(8,128)(2,1)S(1)}, bf16[768,256]{0,1:T(8,128)(2,1)}, u32[]{:S(2)}) copy-start(bf16[768,256]{0,1:T(8,128)(2,1)} %get-tuple-element.21) | copy-start | bytes 1179652
  262.4 24.9 %all-to-all-start.4 = ((bf16[16,256,128]{1,2,0:T(8,128)(2,1)}), bf16[16,256,128]{1,2,0:T(8,128)(2,1)}, u32[]{:S(2)}, u32[]{:S(2)}) async-start(bf16[16,256,128]{1,2,0:T(8,128)(2,1)} %broadcast_in_dim.38), calls=%async_computation.5 | async-start | bytes 2097152 | tf_op jit(solution)/shard_map/all_to_all | solution.py:21
  266.9 1.6 copy-start.1
  266.9 2.2 copy-start.2
  269.1 2.4 copy-start.3
  281.6 5.7 %copy-start.16 = (bf16[256,2048]{1,0:T(8,128)(2,1)S(1)}, bf16[256,2048]{1,0:T(8,128)(2,1)}, u32[]{:S(2)}) copy-start(bf16[256,2048]{1,0:T(8,128)(2,1)} %param.10) | copy-start | bytes 3145732
  281.6 5.7 %copy-start.23 = (f32[2048]{0:T(1024)S(1)}, f32[2048]{0:T(1024)}, u32[]{:S(2)}) copy-start(f32[2048]{0:T(1024)} %param.17) | copy-start | bytes 24580
  (2 other events, 2.6 us)
Sparse Core Ops, SparseCore 0:
  73.4 71.0 all-gather.1
  169.8 42.5 reduce-scatter.1
where the time goes:
time: 302 us; the launch traced here: 296 us
  waiting for transfers between devices  73.4 us (24%)
  local copies, waits for them, and re-layouts  69.5 us (23%)
  blocking collectives  49.1 us (16%)
  matrix products  34.9 us (12%)
  starting transfers between devices  30.9 us (10%)
  other arithmetic  24.1 us (8%)
  between operations  14.6 us (5%)
    all_gather x1, waiting for transfers between devices, side_by_side(): filled, at, done = (lax.all_gather(both, axis, axis=dim, tiled=True), 0, [])  52.1 us
    unnamed x1, blocking collectives  23.5 us
    all_to_all x1, blocking collectives, shards(): lax.all_to_all(cut_cotan, 'ep', split_axis=0, concat_axis=0, tiled=True)  16.6 us
    all_to_all x1, waiting for transfers between devices, summed_on_arrival(): tiles = lax.all_to_all(cut_along(array, dim, peers), axis, 0, 0, tiled=True)  14.4 us
    unnamed x62, local copies, waits for them, and re-layouts  11.2 us
    gather x1, local copies, waits for them, and re-layouts, shards(): jnp.concatenate([route_weights.reshape(routed), jnp.zeros((1,), jnp.bfloa...  9.46 us
    another operation x2, other arithmetic  9.04 us
    all_to_all x1, blocking collectives, shards(): lax.all_to_all(send_weight, 'ep', split_axis=0, concat_axis=0, tiled=True)  9.03 us
  transfers between devices with their start and end apart: 7, of which 4 were waited for; matrix products, arithmetic and copies ran while one was open for 23% of the time, Pallas kernels for 0%

commit v1 on v0

v1 whole, which is shorter than its diff:
```python
import functools

import jax
import jax.numpy as jnp
from jax import lax
from jax.experimental import pallas as pl
from jax.experimental.pallas import tpu as pltpu
from jax.sharding import PartitionSpec as P

clamp_limit = 7.0
sigmoid_slope = 1.702
MESH = pl.DeviceIdType.MESH
BF = jnp.bfloat16
F32 = jnp.float32
SIDE = 4


def place():
    ep, tp = lax.axis_index("ep"), lax.axis_index("tp")
    return ep, tp, tp // 2, lax.rem(tp, 2)


def shifted(ep, d, sign):
    z, x = ep // SIDE, lax.rem(ep, SIDE)
    dz, dx = d // SIDE, lax.rem(d, SIDE)
    if sign < 0:
        dz, dx = SIDE - dz, SIDE - dx
    return lax.rem(z + dz, SIDE) * SIDE + lax.rem(x + dx, SIDE)


def tp_at(y, c):
    return lax.rem(y, 4) * 2 + c


def greet(devices):
    barrier = pltpu.get_barrier_semaphore()
    for device in devices:
        pl.semaphore_signal(barrier, inc=1, device_id=device, device_id_type=MESH)
    pl.semaphore_wait(barrier, len(devices))


def remote(src, dst, send, recv, device):
    return pltpu.make_async_remote_copy(
        src_ref=src, dst_ref=dst, send_sem=send, recv_sem=recv, device_id=device, device_id_type=MESH
    )


def dispatch_kernel(
    n, rows_ref, wsend_ref, dw_ref, r_ref, rw_ref, dwall_ref,
    a_send, a_recv, w_send, w_recv, b_send, b_recv, y_send, y_recv, o_send, o_recv, q_send, q_recv, local,
):
    ep, tp, y, c = place()
    half = rows_ref.shape[3]
    width = dw_ref.shape[1]
    par = lax.rem(y, 2)
    cols = pl.ds(pl.multiple_of(c * half, half), half)
    up, down, mate = (ep, tp_at(y + 1, c)), (ep, tp_at(y + 3, c)), (ep, tp_at(y, 1 - c))
    greet([(shifted(ep, d, 1), tp) for d in range(1, n)] + [up, down, mate])

    def a_copy(d):
        return remote(
            rows_ref.at[shifted(ep, d, 1)], r_ref.at[par, :, ep, :, cols],
            a_send.at[d], a_recv.at[d], (shifted(ep, d, 1), tp),
        )

    def w_copy(d):
        return remote(
            wsend_ref.at[shifted(ep, d, 1)], rw_ref.at[ep], w_send.at[d], w_recv.at[d], (shifted(ep, d, 1), tp)
        )

    def b_copy(d):
        return remote(
            dw_ref, dwall_ref.at[:, pl.ds(pl.multiple_of(ep * width, width), width)],
            b_send.at[d], b_recv.at[d], (shifted(ep, d, 1), tp),
        )

    own_rows = pltpu.make_async_copy(rows_ref.at[ep], r_ref.at[par, :, ep, :, cols], local.at[0])
    own_weight = pltpu.make_async_copy(wsend_ref.at[ep], rw_ref.at[ep], local.at[1])
    own_dense = pltpu.make_async_copy(
        dw_ref, dwall_ref.at[:, pl.ds(pl.multiple_of(ep * width, width), width)], local.at[2]
    )
    own_rows.start()
    own_weight.start()
    own_dense.start()

    @pl.loop(1, n)
    def _(d):
        a_copy(d).start()

    @pl.loop(1, n)
    def _(d):
        w_copy(d).start()
        b_copy(d).start()

    own_rows.wait()
    own_weight.wait()
    own_dense.wait()

    def y_copy(d, e):
        s = shifted(ep, d, -1)
        part = r_ref.at[par, e, s, :, cols]
        return remote(part, part, y_send.at[e, d], y_recv.at[e, d], up if e == 0 else down)

    def o_copy(d):
        part = r_ref.at[par, :, shifted(ep, d, -1), :, cols]
        return remote(part, part, o_send.at[d], o_recv.at[d], mate)

    def q_copy(d, e):
        part = r_ref.at[1 - par, e, shifted(ep, d, -1), :, cols]
        return remote(part, part, q_send.at[e, d], q_recv.at[e, d], mate)

    lag = 3

    @pl.loop(0, n + lag)
    def _(t):
        @pl.when(t < n)
        def _():
            @pl.when(t > 0)
            def _():
                a_copy(t).wait_recv()

            y_copy(t, 0).start()
            y_copy(t, 1).start()
            o_copy(t).start()

        @pl.when(t >= lag)
        def _():
            for e in range(2):
                y_copy(t - lag, e).wait_recv()
                q_copy(t - lag, e).start()

    @pl.loop(0, n)
    def _(d):
        @pl.when(d > 0)
        def _():
            a_copy(d).wait_send()
            w_copy(d).wait()
            b_copy(d).wait()

        o_copy(d).wait()
        for e in range(2):
            y_copy(d, e).wait_send()
            q_copy(d, e).wait()


def dispatch(rows, wsend, dw, n):
    slots = rows.shape[2]
    model = rows.shape[3] * 2
    dma = pltpu.SemaphoreType.DMA
    return pl.pallas_call(
        functools.partial(dispatch_kernel, n),
        out_shape=(
            jax.ShapeDtypeStruct((2, 2, n, slots, model), BF),
            jax.ShapeDtypeStruct(wsend.shape, BF),
            jax.ShapeDtypeStruct((dw.shape[0], dw.shape[1] * n), BF),
        ),
        in_specs=[pl.BlockSpec(memory_space=pl.ANY)] * 3,
        out_specs=[pl.BlockSpec(memory_space=pl.ANY)] * 3,
        scratch_shapes=[
            dma((n,)), dma((n,)), dma((n,)), dma((n,)), dma((n,)), dma((n,)),
            dma((2, n)), dma((2, n)), dma((n,)), dma((n,)), dma((2, n)), dma((2, n)), dma((3,)),
        ],
        compiler_params=pltpu.CompilerParams(collective_id=0, has_side_effects=True),
    )(rows, wsend, dw)


def combine_kernel(
    n, rb_ref, sc_ref, dg_ref, hl_ref, hs_ref, dgall_ref,
    own, mine, yin, tot,
    l_sem, d_send, d_recv, y_send, y_recv, t_send, t_recv, s_send, s_recv, g_send, g_recv, local,
):
    ep, tp, y, c = place()
    block = rb_ref.shape[3] // 8
    width = dgall_ref.shape[2]
    up, down, mate = (ep, tp_at(y + 1, c)), (ep, tp_at(y + 3, c)), (ep, tp_at(y, 1 - c))
    greet([(shifted(ep, d, 1), tp) for d in range(1, n)] + [up, down, mate])

    def at_block(index):
        return pl.ds(pl.multiple_of(index * block, block), block)

    def own_copy(d, j):
        return pltpu.make_async_copy(
            rb_ref.at[:, shifted(ep, d, 1), :, at_block(2 * j + c)], own.at[d, :, :, at_block(j)], l_sem.at[j, d]
        )

    def mate_copy(d, j):
        return remote(
            rb_ref.at[:, shifted(ep, d, 1), :, at_block(2 * j + 1 - c)], mine.at[d, :, :, at_block(j)],
            d_send.at[j, d], d_recv.at[j, d], mate,
        )

    def s_copy(d):
        return remote(sc_ref.at[shifted(ep, d, 1)], hs_ref.at[ep], s_send.at[d], s_recv.at[d], (shifted(ep, d, 1), tp))

    def g_copy(d):
        to = shifted(ep, d, 1)
        return remote(
            dg_ref.at[:, pl.ds(pl.multiple_of(to * width, width), width)], dgall_ref.at[ep],
            g_send.at[d], g_recv.at[d], (to, tp),
        )

    own_score = pltpu.make_async_copy(sc_ref.at[ep], hs_ref.at[ep], local.at[0])
    own_dense = pltpu.make_async_copy(
        dg_ref.at[:, pl.ds(pl.multiple_of(ep * width, width), width)], dgall_ref.at[ep], local.at[1]
    )
    own_score.start()
    own_dense.start()

    @pl.loop(0, n)
    def _(d):
        for j in range(4):
            mate_copy(d, j).start()
            own_copy(d, j).start()

    @pl.loop(1, n)
    def _(d):
        s_copy(d).start()
        g_copy(d).start()

    def y_copy(d, way):
        index = lax.rem(y + 1, 4) if way == 0 else lax.rem(y + 3, 4)
        return remote(
            own.at[d, :, :, at_block(index)], yin.at[way, d], y_send.at[way, d], y_recv.at[way, d],
            up if way == 0 else down,
        )

    def t_copy(d):
        return remote(tot.at[d], hl_ref.at[ep], t_send.at[d], t_recv.at[d], (shifted(ep, d, 1), tp))

    lag = 4

    @pl.loop(0, n + lag)
    def _(t):
        @pl.when(t < n)
        def _():
            for j in range(4):
                own_copy(t, j).wait()
                mate_copy(t, j).wait_recv()
            for e in range(2):
                own[t, e] = (own[t, e].astype(F32) + mine[t, e].astype(F32)).astype(BF)
            y_copy(t, 0).start()
            y_copy(t, 1).start()

        @pl.when(t >= lag)
        def _():
            d = t - lag
            y_copy(d, 0).wait_recv()
            y_copy(d, 1).wait_recv()
            for e in range(2):
                near = own[d, e, :, at_block(y)].astype(F32)
                near = near + yin[0, d, e].astype(F32) + yin[1, d, e].astype(F32)
                tot[d, e, :, 0:block] = near.astype(BF)
                tot[d, e, :, block : 2 * block] = own[d, e, :, at_block(lax.rem(y + 2, 4))]

            @pl.when(d > 0)
            def _():
                t_copy(d).start()

    own_tot = pltpu.make_async_copy(tot.at[0], hl_ref.at[ep], local.at[2])
    own_tot.start()
    own_score.wait()
    own_dense.wait()
    own_tot.wait()

    @pl.loop(0, n)
    def _(d):
        @pl.when(d > 0)
        def _():
            s_copy(d).wait()
            g_copy(d).wait()
            t_copy(d).wait()

        for j in range(4):
            mate_copy(d, j).wait_send()
        for way in range(2):
            y_copy(d, way).wait_send()


def combine(rb, sc, dg, n, width):
    slots, model = rb.shape[2:]
    dma = pltpu.SemaphoreType.DMA
    return pl.pallas_call(
        functools.partial(combine_kernel, n),
        out_shape=(
            jax.ShapeDtypeStruct((n, 2, slots, model // 4), BF),
            jax.ShapeDtypeStruct(sc.shape, BF),
            jax.ShapeDtypeStruct((n, dg.shape[0], width), BF),
        ),
        in_specs=[pl.BlockSpec(memory_space=pl.ANY)] * 3,
        out_specs=[pl.BlockSpec(memory_space=pl.ANY)] * 3,
        scratch_shapes=[
            pltpu.VMEM((n, 2, slots, model // 2), BF),
            pltpu.VMEM((n, 2, slots, model // 2), BF),
            pltpu.VMEM((2, n, 2, slots, model // 8), BF),
            pltpu.VMEM((n, 2, slots, model // 4), BF),
            dma((4, n)), dma((4, n)), dma((4, n)), dma((2, n)), dma((2, n)), dma((n,)), dma((n,)),
            dma((n,)), dma((n,)), dma((n,)), dma((n,)), dma((3,)),
        ],
        compiler_params=pltpu.CompilerParams(collective_id=1, has_side_effects=True),
    )(rb, sc, dg)


def finish_kernel(part_ref, score_ref, got_ref, scores_ref, p_send, p_recv, s_send, s_recv, local):
    ep, tp, y, c = place()
    greet([(ep, lax.rem(tp + k, 8)) for k in range(1, 8)])
    across = remote(part_ref, got_ref, p_send, p_recv, (ep, tp_at(y + 2, c)))
    across.start()
    own = pltpu.make_async_copy(score_ref, scores_ref.at[tp], local)
    own.start()
    copies = [
        remote(score_ref, scores_ref.at[tp], s_send.at[k], s_recv.at[k], (ep, lax.rem(tp + k, 8))) for k in range(1, 8)
    ]
    for copy in copies:
        copy.start()
    own.wait()
    for copy in copies:
        copy.wait()
    across.wait()


def finish(part, score):
    dma = pltpu.SemaphoreType.DMA
    return pl.pallas_call(
        finish_kernel,
        out_shape=(
            jax.ShapeDtypeStruct(part.shape, part.dtype),
            jax.ShapeDtypeStruct((8, *score.shape), score.dtype),
        ),
        in_specs=[pl.BlockSpec(memory_space=pltpu.VMEM)] * 2,
        out_specs=[pl.BlockSpec(memory_space=pltpu.VMEM)] * 2,
        scratch_shapes=[dma, dma, dma((8,)), dma((8,)), dma],
        compiler_params=pltpu.CompilerParams(collective_id=2, has_side_effects=True),
    )(part, score)


def batched(a, b, ca, cb):
    return lax.dot_general(a, b, (((ca,), (cb,)), ((0,), (0,))), preferred_element_type=F32)


def shards(
    tokens, cotangent, expert_ids, route_weights, gate_weight, up_weight, down_weight, dense_weight, dense_gate
):
    tok_rows, model = tokens.shape
    top_count = expert_ids.shape[1]
    local_count = gate_weight.shape[0]
    n = lax.axis_size("ep")
    experts = local_count * n
    slots = tok_rows * top_count * 3 // (2 * experts)
    half, block = model // 2, model // 8
    ep, tp, y, c = place()

    names = expert_ids.T[None] == jnp.arange(experts, dtype=jnp.int32)[:, None, None]
    member = jnp.sum(names.astype(F32), axis=1)
    weight_of = jnp.sum(jnp.where(names, route_weights.T[None].astype(F32), 0.0), axis=1)
    row_at = lax.broadcasted_iota(jnp.int32, (tok_rows, tok_rows), 0)
    col_at = lax.broadcasted_iota(jnp.int32, (tok_rows, tok_rows), 1)
    before = (row_at < col_at).astype(BF)
    rank = jnp.dot(member.astype(BF), before, preferred_element_type=F32)
    rank = jnp.where(member > 0.5, rank, -1.0)
    places = jnp.arange(slots, dtype=jnp.int32).astype(F32)
    picked = rank[:, None, :] == places[None, :, None]
    pick = picked.astype(BF)
    slot_weight = jnp.sum(jnp.where(picked, weight_of[:, None, :], 0.0), axis=2).astype(BF)
    pick_rows = pick.reshape(experts * slots, tok_rows)
    wsend = jnp.pad(slot_weight.reshape(n, local_count, slots), ((0, 0), (0, 16 - local_count), (0, 128 - slots)))

    source = jnp.where(
        lax.rem(y, 2) == 0,
        lax.dynamic_slice_in_dim(tokens, c * half, half, 1),
        lax.dynamic_slice_in_dim(cotangent, c * half, half, 1),
    )
    rows = jnp.dot(pick_rows, source, preferred_element_type=F32).astype(BF)
    rows = rows.reshape(n, local_count, slots, half)

    got, got_weight, dense_all = dispatch(rows, wsend, dense_weight, n)

    gated = (dense_gate[None, :] * cotangent.astype(F32)).astype(BF)
    own_input = lax.dynamic_slice_in_dim(tokens, tp * block, block, 1)
    dense_part = lax.dot_general(
        own_input, gated, (((0,), (0,)), ((), ())), preferred_element_type=F32
    ).astype(BF)

    row_input = got[0].reshape(local_count, n * slots, model)
    row_cotan = got[1].reshape(local_count, n * slots, model)
    row_weight = got_weight[:, :local_count, :slots].transpose(1, 0, 2).reshape(local_count, n * slots, 1).astype(F32)

    gate_pre = batched(row_input, gate_weight, 2, 1)
    up_pre = batched(row_input, up_weight, 2, 1)
    gate_val = jnp.minimum(gate_pre, clamp_limit)
    up_val = jnp.clip(up_pre, -clamp_limit, clamp_limit)
    squash = jax.nn.sigmoid(sigmoid_slope * gate_val)
    hidden = ((up_val + 1.0) * gate_val * squash).astype(BF)
    down_back = batched(row_cotan, down_weight, 2, 2)
    scores = jnp.sum(hidden.astype(F32) * down_back, axis=2)
    hidden_back = row_weight * down_back
    gate_slope = squash + sigmoid_slope * gate_val * squash * (1.0 - squash)
    gate_back = jnp.where(gate_pre < clamp_limit, hidden_back * (up_val + 1.0) * gate_slope, 0.0).astype(BF)
    up_back = jnp.where(jnp.abs(up_pre) < clamp_limit, hidden_back * gate_val * squash, 0.0).astype(BF)
    weighted = (row_weight * row_cotan.astype(F32)).astype(BF)
    back = batched(gate_back, gate_weight, 2, 2) + batched(up_back, up_weight, 2, 2)
    grad_gate = batched(row_input, gate_back, 1, 1)
    grad_up = batched(row_input, up_back, 1, 1)
    grad_down = batched(hidden, weighted, 1, 1)

    back = back.astype(BF).reshape(local_count, n, slots, model)
    score_send = jnp.pad(
        scores.astype(BF).reshape(local_count, n, slots).transpose(1, 0, 2),
        ((0, 0), (0, 16 - local_count), (0, 128 - slots)),
    )
    home, home_score, dense_parts = combine(back, score_send, dense_part, n, model // n)

    both = lax.dot_general(
        pick_rows, home.reshape(experts * slots, 2 * block), (((0,), (0,)), ((), ())), preferred_element_type=F32
    )
    slot_score = home_score[:, :local_count, :slots].reshape(experts, slots, 1).astype(F32)
    of_expert = jnp.sum(jnp.where(picked, slot_score, 0.0), axis=1)
    of_choice = jnp.sum(jnp.where(names, of_expert[:, None, :], 0.0), axis=0)
    score_part = of_choice.reshape(tok_rows * top_count // 128, 128)
    far, all_scores = finish(both[:, block:].astype(BF), score_part)

    dense_back = lax.dot_general(gated, dense_all, (((1,), (1,)), ((), ())), preferred_element_type=F32)
    token_grad = (both[:, :block] + far.astype(F32) + dense_back).astype(BF)
    weight_grad = jnp.sum(all_scores, axis=0).reshape(top_count, tok_rows).T.astype(BF)
    dense_grad = jnp.sum(dense_parts.astype(F32), axis=0)
    return token_grad, weight_grad, grad_gate, grad_up, grad_down, dense_grad


def solution(mesh):
    in_specs = (
        P("ep", None),
        P("ep", None),
        P("ep", None),
        P("ep", None),
        P("ep", None, "tp"),
        P("ep", None, "tp"),
        P("ep", "tp", None),
        P("tp", "ep"),
        P(),
    )
    out_specs = (
        P("ep", "tp"),
        P("ep", None),
        P("ep", None, "tp"),
        P("ep", None, "tp"),
        P("ep", "tp", None),
        P("tp", "ep"),
    )
    return jax.shard_map(shards, mesh=mesh, in_specs=in_specs, out_specs=out_specs, check_vma=False)
```

time: 302 us -> 194 us (0.64); the launches traced: 296 us -> 193 us
  Pallas kernels: 0 us -> 124 us
  waiting for transfers between devices: 73.4 us -> 0 us
  local copies, waits for them, and re-layouts: 69.5 us -> 12.8 us
  blocking collectives: 49.1 us -> 0 us
  starting transfers between devices: 30.9 us -> 0 us
  other arithmetic: 24.1 us -> 5.69 us
  matrix products: 34.9 us -> 50.2 us
  between operations: 14.6 us -> 0.84 us
    pallas_call x0 -> x3, Pallas kernels: none -> 124 us  [the longest x1 69.1 us: dispatch(): pl.pallas_call(functools.partial(dispatch_kernel, n), out_shape=(jax.Shap...]
    all_gather x1 -> x0, waiting for transfers between devices: 52.1 us -> none  [side_by_side(): filled, at, done = (lax.all_gather(both, axis, axis=dim, tiled=True), 0, [])]
    gather x5 -> x0, local copies, waits for them, and re-layouts: 35.2 us -> none  [the longest x1 9.46 us: shards(): jnp.concatenate([route_weights.reshape(routed), jnp.zeros((1,), jnp.bfloa...]
    all_to_all x5 -> x0, starting transfers between devices: 30.8 us -> none  [the longest x1 8.42 us: shards(): lax.all_to_all(cut_input, 'ep', split_axis=0, concat_axis=0, tiled=True)]
    all_to_all x2 -> x0, blocking collectives: 25.6 us -> none  [the longest x1 16.6 us: shards(): lax.all_to_all(cut_cotan, 'ep', split_axis=0, concat_axis=0, tiled=True)]
    unnamed x1 -> x0, blocking collectives: 23.5 us -> none
    all_to_all x5 -> x0, waiting for transfers between devices: 21.3 us -> none  [the longest x1 14.4 us: summed_on_arrival(): tiles = lax.all_to_all(cut_along(array, dim, peers), axis, 0, 0, tiled=True)]
    another operation x7 -> x0, other arithmetic: 19.1 us -> none
  transfers between devices with their start and end apart: 7 -> 0, of which waited for: 4 -> 0; matrix products, arithmetic and copies ran while one was open for 23% -> 0% of each run, Pallas kernels for 0% -> 0%
where the time goes in v1:
time: 194 us; the launch traced here: 193 us
  Pallas kernels  124 us (64%)
  matrix products  50.2 us (26%)
  local copies, waits for them, and re-layouts  12.8 us (7%)
  other arithmetic  5.69 us (3%)
    pallas_call x1, Pallas kernels, dispatch(): pl.pallas_call(functools.partial(dispatch_kernel, n), out_shape=(jax.Shap...  69.1 us
    pallas_call x1, Pallas kernels, combine(): pl.pallas_call(functools.partial(combine_kernel, n), out_shape=(jax.Shape...  45 us
    dot_general x8, matrix products, batched(): lax.dot_general(a, b, (((ca,), (cb,)), ((0,), (0,))), preferred_element_t...  38.8 us
    pallas_call x1, Pallas kernels, finish(): pl.pallas_call(finish_kernel, out_shape=(jax.ShapeDtypeStruct(part.shape,...  9.77 us
    slice x1, local copies, waits for them, and re-layouts, shards(): row_input = got[0].reshape(local_count, n * slots, model)  8.38 us
    dot_general x1, matrix products, shards(): rows = jnp.dot(pick_rows, source, preferred_element_type=F32).astype(BF)  3.89 us

profile of v1, /device:TPU:1, one launch (start us, length us, event | category | flops | bytes accessed | tf_op | source)
XLA Modules:
  0.0 193.5 jit_solution(5169820173091329810)
XLA Ops:
  0.7 0.8 convert_bitcast_fusion.1
  1.5 0.7 select_reduce_fusion.3
  2.2 0.1 convolution_select_fusion
  2.5 0.3 bitcast_compare_fusion
  2.8 3.9 %convolution_convert_fusion = bf16[1536,1024]{1,0:T(8,128)(2,1)} fusion(pred[1536,256]{1,0:T(32,128)(4,1)S(1)} %bitcast_compare_fusion, bf16[256,2048]{1,0:T(8,128)(2,1)} %param.10, s32[]{:T(128)S(6)} %select_n.50, bf16[256,2048]{1,0:T(8,128)(2,1)} %param.9, pred[]{:T(512)S(6)} %eq.61), kind=kOutput, calls=%fused_computation.4 | convolution fusion | flops 807141376 | bytes 4587525 | tf_op jit(solution)/shard_map/dot_general | solution.py:372
  6.6 0.4 select_reduce_fusion.1
  7.0 0.6 pad.7.wsend_ref
  7.7 69.1 %shard_map.136 = (bf16[2,2,16,48,2048]{4,3,2,1,0:T(8,128)(2,1)}, bf16[16,16,128]{2,1,0:T(8,128)(2,1)}, bf16[256,2048]{1,0:T(8,128)(2,1)}) custom-call(bf16[16,2,48,1024]{3,2,1,0:T(8,128)(2,1)} %bitcast.44, bf16[16,16,128]{2,1,0:T(8,128)(2,1)} %pad.7.wsend_ref, bf16[256,128]{1,0:T(8,128)(2,1)} %dw_ref.1), custom_call_target="tpu_custom_call" | custom-call | tf_op jit(solution)/shard_map/pallas_call | solution.py:150
  76.8 8.4 %fusion.13 = (bf16[1,2,16,48,2048]{4,3,2,1,0:T(8,128)(2,1)S(1)}, bf16[1,2,16,48,2048]{4,3,2,1,0:T(8,128)(2,1)}) fusion(bf16[2,2,16,48,2048]{4,3,2,1,0:T(8,128)(2,1)} %get-tuple-element.14), kind=kLoop, calls=%fused_computation.48 | loop fusion | bytes 25165824 | tf_op jit(solution)/shard_map/slice | solution.py:383
  85.2 3.2 %fusion.7 = (u8[768,256]{0,1:T(8,128)(4,1)S(1)}, f32[2,768,256]{1,2,0:T(8,128)}) fusion(bf16[2,768,2048]{2,1,0:T(8,128)(2,1)S(1)} %bitcast.39, bf16[2,2048,256]{2,1,0:T(8,128)(2,1)S(1)} %copy-done), kind=kOutput, calls=%fused_computation.31 | convolution fusion | flops 1612382208 | bytes 10158080 | tf_op jit(solution)/shard_map/dot_general | solution.py:337
  88.4 0.1 copy-done.1
  88.5 3.2 %fusion.8 = (u8[768,256]{0,1:T(8,128)(4,1)S(1)}, f32[2,768,256]{1,2,0:T(8,128)}) fusion(bf16[2,768,2048]{2,1,0:T(8,128)(2,1)S(1)} %bitcast.40, bf16[2,2048,256]{2,1,0:T(8,128)(2,1)S(1)} %copy-done.4), kind=kOutput, calls=%fused_computation.32 | convolution fusion | flops 1612775424 | bytes 10158080 | tf_op jit(solution)/shard_map/dot_general | solution.py:337
  91.7 0.8 convert_bitcast_fusion
  92.5 7.5 %multiply_reduce_fusion = (bf16[2,768]{1,0:T(2,128)(2,1)S(1)}, bf16[2,768,256]{1,2,0:T(8,128)(2,1)S(1)}, bf16[2,768,256]{1,2,0:T(8,128)(2,1)S(1)}, bf16[2,768,256]{1,2,0:T(8,128)(2,1)S(1)}) fusion(f32[2,768,256]{1,2,0:T(8,128)} %get-tuple-element.31, f32[2,768,256]{1,2,0:T(8,128)} %get-tuple-element.33, f32[2,768]{1,0:T(2,128)S(1)} %reshape.100, ...), kind=kOutput, calls=%fused_computation.15 | convolution fusion | flops 1623587328 | bytes 14296064 | tf_op jit(solution)/shard_map/dot_general | solution.py:337
  100.1 7.0 %fusion = f32[2,256,2048]{2,1,0:T(8,128)} fusion(bf16[2,768,256]{1,2,0:T(8,128)(2,1)S(1)} %get-tuple-element.25, bf16[2,768,2048]{2,1,0:T(8,128)(2,1)} %bitcast.46, f32[2,768]{1,0:T(2,128)S(1)} %reshape.100), kind=kOutput, calls=%fused_computation.2 | convolution fusion | flops 1620049920 | bytes 11278336 | tf_op jit(solution)/shard_map/dot_general | solution.py:337
  107.0 4.6 %fusion.17 = f32[2,2048,256]{2,1,0:T(8,128)} fusion(bf16[2,768,2048]{2,1,0:T(8,128)(2,1)S(1)} %bitcast.41, bf16[2,768,256]{1,2,0:T(8,128)(2,1)S(1)} %get-tuple-element.29), kind=kOutput, calls=%fused_computation.52 | convolution fusion | flops 1610612736 | bytes 11272192 | tf_op jit(solution)/shard_map/dot_general | solution.py:337
  111.6 4.8 %fusion.16 = f32[2,2048,256]{2,1,0:T(8,128)} fusion(bf16[2,768,2048]{2,1,0:T(8,128)(2,1)S(1)} %bitcast.42, bf16[2,768,256]{1,2,0:T(8,128)(2,1)S(1)} %get-tuple-element.28), kind=kOutput, calls=%fused_computation.51 | convolution fusion | flops 1610612736 | bytes 11272192 | tf_op jit(solution)/shard_map/dot_general | solution.py:337
  116.4 2.0 %fusion.14 = f32[2,768,2048]{2,1,0:T(8,128)S(1)} fusion(bf16[2,768,256]{1,2,0:T(8,128)(2,1)S(1)} %get-tuple-element.28, bf16[2,2048,256]{2,1,0:T(8,128)(2,1)S(1)} %copy-done), kind=kOutput, calls=%fused_computation.49 | convolution fusion | flops 1610612736 | bytes 15466496 | tf_op jit(solution)/shard_map/dot_general | solution.py:337
  118.4 6.6 %add_convert_fusion = bf16[2,768,2048]{2,1,0:T(8,128)(2,1)} fusion(f32[2,768,2048]{2,1,0:T(8,128)S(1)} %fusion.14, bf16[2,768,256]{1,2,0:T(8,128)(2,1)S(1)} %get-tuple-element.29, bf16[2,2048,256]{2,1,0:T(8,128)(2,1)} %param.14), kind=kOutput, calls=%fused_computation.1 | convolution fusion | flops 1616904192 | bytes 21757952 | tf_op jit(solution)/shard_map/dot_general | solution.py:337
  125.1 0.6 pad.8.sc_ref
  125.8 2.8 %convolution_convert_fusion.1.dg_ref = bf16[256,2048]{1,0:T(8,128)(2,1)} fusion(bf16[256,2048]{1,0:T(8,128)(2,1)} %param.10, f32[2048]{0:T(1024)S(1)} %copy-done.8, bf16[256,2048]{1,0:T(8,128)(2,1)} %param.9, s32[]{:T(128)S(6)} %select_n.56), kind=kOutput, calls=%fused_computation.5 | convolution fusion | flops 270532608 | bytes 2236420 | tf_op jit(solution)/shard_map/dot_general | solution.py:379
  128.6 45.0 %shard_map.137 = (bf16[16,2,48,512]{3,2,1,0:T(8,128)(2,1)}, bf16[16,16,128]{2,1,0:T(8,128)(2,1)}, bf16[16,256,128]{2,1,0:T(8,128)(2,1)}) custom-call(bf16[2,16,48,2048]{3,2,1,0:T(8,128)(2,1)} %bitcast.43, bf16[16,16,128]{2,1,0:T(8,128)(2,1)} %pad.8.sc_ref, bf16[256,2048]{1,0:T(8,128)(2,1)} %convolution_convert_fusion.1.dg_ref), custom_call_target="tpu_custom_call" | custom-call | tf_op jit(solution)/shard_map/pallas_call | solution.py:282
  173.6 0.3 broadcast_compare_fusion
  173.9 2.1 %fusion.15 = f32[256,512]{1,0:T(8,128)S(1)} fusion(pred[1536,256]{1,0:T(8,128)(4,1)S(1)} %bitcast.47, bf16[1536,512]{1,0:T(8,128)(2,1)} %bitcast.54), kind=kOutput, calls=%fused_computation.50 | convolution fusion | flops 402653184 | bytes 2490368 | tf_op jit(solution)/shard_map/dot_general | solution.py:412
  176.0 0.7 slice.32.part_ref
  176.8 0.8 slice.24
  177.6 0.4 select_reduce_fusion
  178.0 0.6 reshape.99.score_ref
  178.6 9.8 %shard_map.138 = (bf16[256,256]{1,0:T(8,128)(2,1)}, f32[8,8,128]{2,1,0:T(8,128)}) custom-call(bf16[256,256]{1,0:T(8,128)(2,1)} %slice.32.part_ref, f32[8,128]{1,0:T(8,128)} %reshape.99.score_ref), custom_call_target="tpu_custom_call" | custom-call | tf_op jit(solution)/shard_map/pallas_call | solution.py:323
  188.4 2.4 %fusion.2 = bf16[256,256]{1,0:T(8,128)(2,1)} fusion(bf16[256,2048]{1,0:T(8,128)(2,1)} %get-tuple-element.19, bf16[256,2048]{1,0:T(8,128)(2,1)S(1)} %copy-done.3, f32[2048]{0:T(1024)S(1)} %copy-done.8, f32[256,512]{1,0:T(8,128)} %copy-done.5, bf16[256,256]{1,0:T(8,128)(2,1)} %get-tuple-element.18), kind=kOutput, calls=%fused_computation.24 | convolution fusion | flops 270270464 | bytes 2629632 | tf_op jit(solution)/shard_map/dot_general | solution.py:421
  190.8 0.6 convert_element_type.144
  191.4 2.0 %convert_reduce_fusion = f32[256,128]{1,0:T(8,128)} fusion(bf16[16,256,128]{2,1,0:T(8,128)(2,1)} %get-tuple-element.21), kind=kLoop, calls=%fused_computation.6 | loop fusion | flops 1015808 | bytes 1179648 | tf_op jit(solution)/shard_map/reduce_sum | solution.py:424
  (27 shorter events, 0.4 us)
Async XLA Ops:
  0.6 84.5 %copy-start = (bf16[2,2048,256]{2,1,0:T(8,128)(2,1)S(1)}, bf16[2,2048,256]{2,1,0:T(8,128)(2,1)}, u32[]{:S(2)}) copy-start(bf16[2,2048,256]{2,1,0:T(8,128)(2,1)} %param.13) | copy-start | bytes 6291460
  85.2 3.3 %copy-start.1 = (bf16[1,2,16,48,2048]{4,3,2,1,0:T(8,128)(2,1)}, bf16[1,2,16,48,2048]{4,3,2,1,0:T(8,128)(2,1)S(1)}, u32[]{:S(2)}) copy-start(bf16[1,2,16,48,2048]{4,3,2,1,0:T(8,128)(2,1)S(1)} %get-tuple-element.26) | copy-start | bytes 18874372
  85.2 3.3 %copy-start.4 = (bf16[2,2048,256]{2,1,0:T(8,128)(2,1)S(1)}, bf16[2,2048,256]{2,1,0:T(8,128)(2,1)}, u32[]{:S(2)}) copy-start(bf16[2,2048,256]{2,1,0:T(8,128)(2,1)} %param.14) | copy-start | bytes 6291460
  100.0 7.0 %copy-start.2 = (bf16[1,2,16,48,2048]{4,3,2,1,0:T(8,128)(2,1)S(1)}, bf16[1,2,16,48,2048]{4,3,2,1,0:T(8,128)(2,1)}, u32[]{:S(2)}) copy-start(bf16[1,2,16,48,2048]{4,3,2,1,0:T(8,128)(2,1)} %copy-done.1) | copy-start | bytes 18874372
  118.4 7.3 %copy-start.8 = (f32[2048]{0:T(1024)S(1)}, f32[2048]{0:T(1024)}, u32[]{:S(2)}) copy-start(f32[2048]{0:T(1024)} %param.17) | copy-start | bytes 24580
  173.6 4.3 %copy-start.7 = (s32[256,4]{0,1:T(4,128)S(1)}, s32[256,4]{0,1:T(4,128)}, u32[]{:S(2)}) copy-start(s32[256,4]{0,1:T(4,128)} %param.11) | copy-start | bytes 12292
  173.9 14.5 %copy-start.3 = (bf16[256,2048]{1,0:T(8,128)(2,1)S(1)}, bf16[256,2048]{1,0:T(8,128)(2,1)}, u32[]{:S(2)}) copy-start(bf16[256,2048]{1,0:T(8,128)(2,1)} %param.10) | copy-start | bytes 3145732
  176.0 1.9 copy-start.5
  188.4 2.5 %copy-start.6 = (f32[8,8,128]{2,1,0:T(8,128)S(1)}, f32[8,8,128]{2,1,0:T(8,128)}, u32[]{:S(2)}) copy-start(f32[8,8,128]{2,1,0:T(8,128)} %get-tuple-element.20) | copy-start | bytes 98308

commit v2 on v0

v2 whole, which is shorter than its diff:
```python
import functools

import jax
import jax.numpy as jnp
from jax import lax
from jax.experimental import pallas as pl
from jax.experimental.pallas import tpu as pltpu
from jax.sharding import PartitionSpec as P

clamp_limit = 7.0
sigmoid_slope = 1.702
MESH = pl.DeviceIdType.MESH
BF = jnp.bfloat16
F32 = jnp.float32
SIDE = 4
ORDER = (
    (0, 0), (0, 1), (1, 0), (0, 3), (3, 0), (1, 1), (3, 3), (1, 3),
    (3, 1), (0, 2), (2, 0), (2, 2), (1, 2), (2, 1), (3, 2), (2, 3),
)
GROUP = 8
LAG = 3


def place():
    ep, tp = lax.axis_index("ep"), lax.axis_index("tp")
    return ep, tp, tp // 2, lax.rem(tp, 2)


def shifted(ep, step, sign):
    z, x = ep // SIDE, lax.rem(ep, SIDE)
    dz, dx = step
    if sign < 0:
        dz, dx = SIDE - dz, SIDE - dx
    return lax.rem(z + dz, SIDE) * SIDE + lax.rem(x + dx, SIDE)


def tp_at(y, c):
    return lax.rem(y, 4) * 2 + c


def greet(devices):
    barrier = pltpu.get_barrier_semaphore()
    for device in devices:
        pl.semaphore_signal(barrier, inc=1, device_id=device, device_id_type=MESH)
    pl.semaphore_wait(barrier, len(devices))


def remote(src, dst, send, recv, device):
    return pltpu.make_async_remote_copy(
        src_ref=src, dst_ref=dst, send_sem=send, recv_sem=recv, device_id=device, device_id_type=MESH
    )


def nn(a, b):
    return lax.dot_general(a, b, (((1,), (0,)), ((), ())), preferred_element_type=F32)


def nt(a, b):
    return lax.dot_general(a, b, (((1,), (1,)), ((), ())), preferred_element_type=F32)


def tn(a, b):
    return lax.dot_general(a, b, (((0,), (0,)), ((), ())), preferred_element_type=F32)


def exchange_kernel(
    n, rows_ref, weight_ref, wg_ref, wu_ref, wd_ref, tok_ref, cot_ref, scale_ref, dw_ref, pick_ref,
    held_ref, act_out, token_ref, home_score, dense_out,
    r, rw, wg, wu, wd, act, back, mine, part, first, second, total, home, score, scores, to_home,
    tok, cot, pick, dsend, dland, dwall,
    a_send, a_recv, w_send, w_recv, b_send, b_recv, g_send, g_recv,
    y_send, y_recv, o_send, o_recv, q_send, q_recv, d_send, d_recv, f_send, f_recv, h_send, h_recv,
    t_send, t_recv, s_send, s_recv, k_send, k_recv, load, local, out_sem,
):
    ep, tp, y, c = place()
    slots, half = rows_ref.shape[2:]
    quarter, block, width = half // 2, half // 4, dw_ref.shape[1]
    rows = GROUP * slots
    par = lax.rem(y, 2)
    up, down, mate = (ep, tp_at(y + 1, c)), (ep, tp_at(y + 3, c)), (ep, tp_at(y, 1 - c))
    others = [(ep, lax.rem(tp + k, 8)) for k in range(1, 8)]
    targets = [shifted(ep, step, 1) for step in ORDER]
    homes = [shifted(ep, step, -1) for step in ORDER]

    def columns(start, size):
        return pl.ds(pl.multiple_of(start, 128), size)

    mine_cols = columns(c * half, half)
    ep_cols = columns(ep * width, width)

    loads = [
        pltpu.make_async_copy(a, b, load.at[k])
        for k, (a, b) in enumerate(
            [
                (tok_ref.at[:, columns(tp * block, block)], tok),
                (cot_ref, cot),
                (wg_ref, wg),
                (wu_ref, wu),
                (wd_ref, wd),
                (pick_ref, pick),
                (dw_ref, dwall.at[:, ep_cols]),
                (weight_ref.at[ep], rw.at[0]),
                (rows_ref.at[ep, 0], r.at[par, 0, 0, :, mine_cols]),
                (rows_ref.at[ep, 1], r.at[par, 1, 0, :, mine_cols]),
            ]
        )
    ]
    for copy in loads:
        copy.start()
    greet([(targets[i], tp) for i in range(1, n)] + others + [up, down])

    def a_copy(e, i, to):
        return remote(
            rows_ref.at[to, e], r.at[par, e, i, :, mine_cols], a_send.at[e, i], a_recv.at[e, i], (to, tp)
        )

    def w_copy(i):
        return remote(weight_ref.at[targets[i]], rw.at[i], w_send.at[i], w_recv.at[i], (targets[i], tp))

    def b_copy(i):
        return remote(dw_ref, dwall.at[:, ep_cols], b_send.at[i], b_recv.at[i], (targets[i], tp))

    def g_copy(i):
        return remote(
            dsend.at[:, columns(targets[i] * width, width)], dland.at[i], g_send.at[i], g_recv.at[i], (targets[i], tp)
        )

    for i in range(1, n):
        w_copy(i).start()
    for e in range(2):
        for i in range(1, n):
            a_copy(e, i, targets[i]).start()
    for i in range(1, n):
        b_copy(i).start()

    loads[0].wait()
    loads[1].wait()
    cot[...] = (scale_ref[...] * cot[...].astype(F32)).astype(BF)
    for k in range(4):
        dsend[:, k * half // 2 : (k + 1) * half // 2] = tn(
            tok[...], cot[:, k * half // 2 : (k + 1) * half // 2]
        ).astype(BF)
    dland[0] = dsend[:, ep_cols]
    for i in range(1, n):
        g_copy(i).start()
    for copy in loads[2:]:
        copy.wait()
    for i in range(1, n):
        w_copy(i).wait_recv()

    def y_copy(e, i, way):
        piece = r.at[par, e, i, :, columns(c * half + way * quarter, quarter)]
        return remote(piece, piece, y_send.at[way, e, i], y_recv.at[way, e, i], up if way == 0 else down)

    def o_copy(e, i):
        piece = r.at[par, e, i, :, mine_cols]
        return remote(piece, piece, o_send.at[e, i], o_recv.at[e, i], mate)

    def q_copy(e, i, way):
        piece = r.at[1 - par, e, i, :, columns(c * half + way * quarter, quarter)]
        return remote(piece, piece, q_send.at[way, e, i], q_recv.at[way, e, i], mate)

    def serve(t):
        @pl.when(t < 2 * n)
        def _():
            e, i = t // n, lax.rem(t, n)

            @pl.when(i > 0)
            def _():
                a_copy(e, i, targets[1]).wait_recv()

            y_copy(e, i, 0).start()
            y_copy(e, i, 1).start()
            o_copy(e, i).start()

        @pl.when(t >= LAG)
        def _():
            e, i = (t - LAG) // n, lax.rem(t - LAG, n)
            for way in range(2):
                y_copy(e, i, way).wait_recv()
                q_copy(e, i, way).start()

    def group(q):
        return q // 2, pl.ds(lax.rem(q, 2) * GROUP, GROUP)

    def ready(q):
        e = q // 2

        @pl.loop(0, GROUP)
        def _(k):
            i = lax.rem(q, 2) * GROUP + k
            o_copy(e, i).wait_recv()
            for way in range(2):
                q_copy(e, i, way).wait_recv()

    diagonal = lax.broadcasted_iota(jnp.int32, (slots, 128), 0) == lax.broadcasted_iota(jnp.int32, (slots, 128), 1)

    def expert_rows(q):
        e, who = group(q)
        x = r[0, e, who].reshape(rows, 2 * half)
        cotan = r[1, e, who].reshape(rows, 2 * half)
        gate_pre = nn(x, wg[e])
        up_pre = nn(x, wu[e])
        down_back = nt(cotan, wd[e])
        lanes = jnp.where(e == 0, rw[who, 0, :], rw[who, 1, :])
        weight = jnp.sum(jnp.where(diagonal[None], lanes[:, None, :], 0.0), axis=2, keepdims=True).reshape(rows, 1)
        gate_val = jnp.minimum(gate_pre, clamp_limit)
        up_val = jnp.clip(up_pre, -clamp_limit, clamp_limit)
        squash = jax.nn.sigmoid(sigmoid_slope * gate_val)
        swish = gate_val * squash
        hidden = ((up_val + 1.0) * swish).astype(BF).astype(F32)
        row_score = jnp.sum(hidden * down_back, axis=1, keepdims=True).reshape(GROUP, slots, 1)
        score[pl.ds(pl.multiple_of(q * GROUP, GROUP), GROUP), :] = jnp.sum(
            jnp.where(diagonal[None], row_score, 0.0), axis=1
        )
        hidden_back = weight * down_back
        slope = squash + sigmoid_slope * swish * (1.0 - squash)
        act[0, q] = (weight * hidden).astype(BF)
        act[1, q] = jnp.where(gate_pre < clamp_limit, hidden_back * (up_val + 1.0) * slope, 0.0).astype(BF)
        act[2, q] = jnp.where(jnp.abs(up_pre) < clamp_limit, hidden_back * swish, 0.0).astype(BF)
        for k in range(4):
            cols = pl.ds(k * half // 2, half // 2)
            value = nt(act[1, q], wg[e, cols, :]) + nt(act[2, q], wu[e, cols, :])
            back[q, :, cols] = value.astype(BF)

    def d_copy(q, j):
        return remote(
            back.at[q, :, columns((2 * j + 1 - c) * block, block)], mine.at[q, :, pl.ds(j * block, block)],
            d_send.at[j, q], d_recv.at[j, q], mate,
        )

    def f_copy(q, way):
        start = lax.rem(y + 2, 4) * block + way * (block // 2)
        return remote(
            part.at[q, :, columns(start, block // 2)], first.at[way, q], f_send.at[way, q], f_recv.at[way, q],
            up if way == 0 else down,
        )

    def h_copy(q, way):
        start = lax.rem(y + (1 if way == 0 else 3), 4) * block
        return remote(
            part.at[q, :, columns(start, block)], second.at[way, q], h_send.at[way, q], h_recv.at[way, q],
            up if way == 0 else down,
        )

    def t_copy(q, k, to):
        i = lax.rem(q, 2) * GROUP + k
        return remote(
            total.at[q, pl.ds(k * slots, slots)], home.at[ep, q // 2], t_send.at[q, k], t_recv.at[q, k], (to, tp)
        )

    def own_total(e):
        return pltpu.make_async_copy(total.at[2 * e, pl.ds(0, slots)], home.at[ep, e], local.at[e])

    def core_sum(q):
        for j in range(4):
            d_copy(q, j).wait_recv()
        for j in range(4):
            cols = pl.ds(j * block, block)
            both = back[q, :, columns((2 * j + c) * block, block)].astype(F32) + mine[q, :, cols].astype(F32)
            part[q, :, cols] = both.astype(BF)
        for way in range(2):
            f_copy(q, way).start()

    def ring_sum(q):
        for way in range(2):
            f_copy(q, way).wait_recv()
        for way in range(2):
            start = lax.rem(y + (1 if way == 0 else 3), 4) * block + way * (block // 2)
            cols = columns(start, block // 2)
            part[q, :, cols] = (part[q, :, cols].astype(F32) + first[way, q].astype(F32)).astype(BF)
        for way in range(2):
            h_copy(q, way).start()

    def home_sum(q):
        for way in range(2):
            h_copy(q, way).wait_recv()
        value = part[q, :, columns(y * block, block)].astype(F32)
        total[q] = (value + second[0, q].astype(F32) + second[1, q].astype(F32)).astype(BF)
        for k in range(GROUP):
            to = jnp.where(lax.rem(q, 2) == 0, homes[k], homes[GROUP + k])
            if k == 0:

                @pl.when(lax.rem(q, 2) == 0)
                def _():
                    own_total(q // 2).start()

                @pl.when(lax.rem(q, 2) == 1)
                def _():
                    t_copy(q, 0, homes[GROUP]).start()

            else:
                t_copy(q, k, to).start()

    def held_copy(a, e):
        return pltpu.make_async_copy(r.at[a, e], held_ref.at[a, e], out_sem.at[a, e])

    def act_copy(q):
        return pltpu.make_async_copy(act.at[:, q], act_out.at[:, q], out_sem.at[2, q])

    def score_copy(k):
        return remote(score, scores.at[tp], s_send.at[k], s_recv.at[k], (ep, lax.rem(tp + k, 8)))

    def k_copy(i):
        return remote(to_home.at[i], home_score.at[ep], k_send.at[i], k_recv.at[i], (homes[i], tp))

    @pl.loop(0, 7)
    def _(q):
        start = jnp.where(q == 0, 0, jnp.minimum(q * GROUP + 2 * LAG, 2 * n + LAG))
        stop = jnp.where(q >= 3, 2 * n + LAG, (q + 1) * GROUP + 2 * LAG)
        start = jnp.where(q >= 4, 2 * n + LAG, start)
        pl.loop(start, stop)(serve)

        @pl.when((q >= 1) & (q < 5))
        def _():
            core_sum(q - 1)

        @pl.when((q >= 2) & (q < 6))
        def _():
            ring_sum(q - 2)

        @pl.when(q >= 3)
        def _():
            home_sum(q - 3)

        @pl.when(q < 4)
        def _():
            ready(q)
            expert_rows(q)
            for j in range(4):
                d_copy(q, j).start()
            act_copy(q).start()

            @pl.when(lax.rem(q, 2) == 1)
            def _():
                held_copy(0, q // 2).start()
                held_copy(1, q // 2).start()

        @pl.when(q == 3)
        def _():
            for k in range(1, 8):
                score_copy(k).start()
            scores[tp] = score[...]

        @pl.when(q == 4)
        def _():
            for k in range(1, 8):
                score_copy(k).wait_recv()
            every = scores[0]
            for k in range(1, 8):
                every = every + scores[k]
            lower = lax.broadcasted_iota(jnp.int32, (8, 128), 0) == 0
            for i in range(n):
                to_home[i] = jnp.where(lower, every[i : i + 1, :], every[n + i : n + i + 1, :])
            pltpu.make_async_copy(to_home.at[0], home_score.at[ep], local.at[2]).start()
            for i in range(1, n):
                k_copy(i).start()

    for i in range(1, n):
        b_copy(i).wait()
        g_copy(i).wait()
    dense = dland[0].astype(F32)
    for i in range(1, n):
        dense = dense + dland[i].astype(F32)
    dense_out[...] = dense
    back_dense = nt(cot[...], dwall[...])

    own_total(0).wait()
    own_total(1).wait()
    for q in range(4):
        for k in range(GROUP):
            if k > 0 or q % 2 == 1:
                t_copy(q, k, homes[1]).wait_recv()
    got = tn(pick[...], home[...].reshape(n * 2 * slots, block))
    token_ref[...] = (got + back_dense).astype(BF)

    pltpu.make_async_copy(to_home.at[0], home_score.at[ep], local.at[2]).wait()
    for e in range(2):
        for i in range(n):
            if i > 0:
                a_copy(e, i, targets[i]).wait_send()
            o_copy(e, i).wait_send()
            for way in range(2):
                y_copy(e, i, way).wait_send()
                q_copy(e, i, way).wait_send()
    for i in range(1, n):
        w_copy(i).wait_send()
        k_copy(i).wait()
    for k in range(1, 8):
        score_copy(k).wait_send()
    for q in range(4):
        act_copy(q).wait()
        for j in range(4):
            d_copy(q, j).wait_send()
        for way in range(2):
            f_copy(q, way).wait_send()
            h_copy(q, way).wait_send()
        for k in range(GROUP):
            if k > 0 or q % 2 == 1:
                t_copy(q, k, homes[1]).wait_send()
    for e in range(2):
        held_copy(0, e).wait()
        held_copy(1, e).wait()


def exchange(rows, weights, wg, wu, wd, tokens, cotangent, scale, dw, pick):
    n, _, slots, half = rows.shape
    model, block, width = 2 * half, half // 4, dw.shape[1]
    tok_rows = tokens.shape[0]
    units = wg.shape[2]
    dma, vmem = pltpu.SemaphoreType.DMA, pltpu.VMEM
    many = GROUP * slots
    any_space, in_vmem = pl.BlockSpec(memory_space=pl.ANY), pl.BlockSpec(memory_space=vmem)
    return pl.pallas_call(
        functools.partial(exchange_kernel, n),
        out_shape=(
            jax.ShapeDtypeStruct((2, 2, n, slots, model), BF),
            jax.ShapeDtypeStruct((3, 4, many, units), BF),
            jax.ShapeDtypeStruct((tok_rows, block), BF),
            jax.ShapeDtypeStruct(weights.shape, F32),
            jax.ShapeDtypeStruct((block, width), F32),
        ),
        in_specs=[any_space] * 7 + [in_vmem] + [any_space] * 2,
        out_specs=[any_space, any_space, in_vmem, any_space, in_vmem],
        scratch_shapes=[
            vmem((2, 2, n, slots, model), BF),
            vmem(weights.shape, F32),
            vmem(wg.shape, BF),
            vmem(wu.shape, BF),
            vmem(wd.shape, BF),
            vmem((3, 4, many, units), BF),
            vmem((4, many, model), BF),
            vmem((4, many, half), BF),
            vmem((4, many, half), BF),
            vmem((2, 4, many, block // 2), BF),
            vmem((2, 4, many, block), BF),
            vmem((4, many, block), BF),
            vmem((n, 2, slots, block), BF),
            vmem((2 * n, 128), F32),
            vmem((8, 2 * n, 128), F32),
            vmem(weights.shape, F32),
            vmem((tok_rows, block), BF),
            vmem(cotangent.shape, BF),
            vmem(pick.shape, BF),
            vmem((block, model), BF),
            vmem((n, block, width), BF),
            vmem((block, model), BF),
            dma((2, n)), dma((2, n)), dma((n,)), dma((n,)), dma((n,)), dma((n,)), dma((n,)), dma((n,)),
            dma((2, 2, n)), dma((2, 2, n)), dma((2, n)), dma((2, n)), dma((2, 2, n)), dma((2, 2, n)),
            dma((4, 4)), dma((4, 4)), dma((2, 4)), dma((2, 4)), dma((2, 4)), dma((2, 4)),
            dma((4, GROUP)), dma((4, GROUP)), dma((8,)), dma((8,)), dma((n,)), dma((n,)),
            dma((10,)), dma((3,)), dma((3, 4)),
        ],
        compiler_params=pltpu.CompilerParams(collective_id=0, has_side_effects=True, vmem_limit_bytes=62 << 20),
    )(rows, weights, wg, wu, wd, tokens, cotangent, scale, dw, pick)


def gradient_kernel(x_ref, c_ref, act_ref, gate_ref, up_ref, down_ref):
    x, cotan = x_ref[0, 0], c_ref[0, 0]
    many = act_ref.shape[2] * act_ref.shape[1]
    hidden, gate_back, up_back = (act_ref[k].reshape(many, act_ref.shape[3]) for k in range(3))
    gate_ref[0] = tn(x, gate_back)
    up_ref[0] = tn(x, up_back)
    down_ref[0] = tn(hidden, cotan)


def gradients(held, act):
    _, experts, many, model = held.shape
    units = act.shape[3]
    chunk = model // 4
    return pl.pallas_call(
        gradient_kernel,
        grid=(experts, model // chunk),
        out_shape=(
            jax.ShapeDtypeStruct((experts, model, units), F32),
            jax.ShapeDtypeStruct((experts, model, units), F32),
            jax.ShapeDtypeStruct((experts, units, model), F32),
        ),
        in_specs=[
            pl.BlockSpec((1, 1, many, chunk), lambda e, k: (0, e, 0, k)),
            pl.BlockSpec((1, 1, many, chunk), lambda e, k: (1, e, 0, k)),
            pl.BlockSpec((3, 2, many // 2, units), lambda e, k: (0, e, 0, 0)),
        ],
        out_specs=[
            pl.BlockSpec((1, chunk, units), lambda e, k: (e, k, 0)),
            pl.BlockSpec((1, chunk, units), lambda e, k: (e, k, 0)),
            pl.BlockSpec((1, units, chunk), lambda e, k: (e, 0, k)),
        ],
    )(held, held, act)


def shards(
    tokens, cotangent, expert_ids, route_weights, gate_weight, up_weight, down_weight, dense_weight, dense_gate
):
    tok_rows, model = tokens.shape
    top_count = expert_ids.shape[1]
    local_count = gate_weight.shape[0]
    n = lax.axis_size("ep")
    experts = local_count * n
    slots = tok_rows * top_count * 3 // (2 * experts)
    half, block = model // 2, model // 8
    ep, tp, y, c = place()

    names = expert_ids.T[None] == jnp.arange(experts, dtype=jnp.int32)[:, None, None]
    member = jnp.sum(names.astype(F32), axis=1)
    weight_of = jnp.sum(jnp.where(names, route_weights.T[None].astype(F32), 0.0), axis=1)
    row_at = lax.broadcasted_iota(jnp.int32, (tok_rows, tok_rows), 0)
    col_at = lax.broadcasted_iota(jnp.int32, (tok_rows, tok_rows), 1)
    before = (row_at < col_at).astype(BF)
    rank = jnp.dot(member.astype(BF), before, preferred_element_type=F32)
    rank = jnp.where(member > 0.5, rank, -1.0)
    places = jnp.arange(slots, dtype=jnp.int32).astype(F32)
    picked = rank[:, None, :] == places[None, :, None]
    pick = picked.astype(BF)
    slot_weight = jnp.sum(jnp.where(picked, weight_of[:, None, :], 0.0), axis=2)
    pick_rows = pick.reshape(experts * slots, tok_rows)
    weights = jnp.pad(slot_weight.reshape(n, local_count, slots), ((0, 0), (0, 8 - local_count), (0, 128 - slots)))

    source = jnp.where(
        lax.rem(y, 2) == 0,
        lax.dynamic_slice_in_dim(tokens, c * half, half, 1),
        lax.dynamic_slice_in_dim(cotangent, c * half, half, 1),
    )
    rows = jnp.dot(pick_rows, source, preferred_element_type=F32).astype(BF)
    rows = rows.reshape(n, local_count, slots, half)

    held, act, token_grad, home_score, dense_grad = exchange(
        rows, weights, gate_weight, up_weight, down_weight, tokens, cotangent, dense_gate[None, :], dense_weight, pick_rows
    )
    grad_gate, grad_up, grad_down = gradients(held.reshape(2, local_count, n * slots, model), act)

    slot_score = home_score[:, :local_count, :slots].reshape(experts, slots, 1)
    of_expert = jnp.sum(jnp.where(picked, slot_score, 0.0), axis=1)
    of_choice = jnp.sum(jnp.where(names, of_expert[:, None, :], 0.0), axis=0)
    weight_grad = of_choice.T.astype(BF)
    return token_grad, weight_grad, grad_gate, grad_up, grad_down, dense_grad


def solution(mesh):
    in_specs = (
        P("ep", None),
        P("ep", None),
        P("ep", None),
        P("ep", None),
        P("ep", None, "tp"),
        P("ep", None, "tp"),
        P("ep", "tp", None),
        P("tp", "ep"),
        P(),
    )
    out_specs = (
        P("ep", "tp"),
        P("ep", None),
        P("ep", None, "tp"),
        P("ep", None, "tp"),
        P("ep", "tp", None),
        P("tp", "ep"),
    )
    return jax.shard_map(shards, mesh=mesh, in_specs=in_specs, out_specs=out_specs, check_vma=False)
```

time: 302 us -> 128 us (0.42); the launches traced: 296 us -> 127 us
  Pallas kernels: 0 us -> 115 us
  waiting for transfers between devices: 73.4 us -> 0 us
  local copies, waits for them, and re-layouts: 69.5 us -> 2.89 us
  blocking collectives: 49.1 us -> 0 us
  matrix products: 34.9 us -> 3.88 us
  starting transfers between devices: 30.9 us -> 0 us
  other arithmetic: 24.1 us -> 4.05 us
  between operations: 14.6 us -> 0.71 us
    pallas_call x0 -> x2, Pallas kernels: none -> 115 us  [the longest x1 101 us: exchange(): pl.pallas_call(functools.partial(exchange_kernel, n), out_shape=(jax.Shap...]
    all_gather x1 -> x0, waiting for transfers between devices: 52.1 us -> none  [side_by_side(): filled, at, done = (lax.all_gather(both, axis, axis=dim, tiled=True), 0, [])]
    gather x5 -> x0, local copies, waits for them, and re-layouts: 35.2 us -> none  [the longest x1 9.46 us: shards(): jnp.concatenate([route_weights.reshape(routed), jnp.zeros((1,), jnp.bfloa...]
    dot_general x18 -> x2, matrix products: 34.9 us -> 3.88 us  [the longest x1 3.73 us: shards(): rows = jnp.dot(pick_rows, source, preferred_element_type=F32).astype(BF)]
    all_to_all x5 -> x0, starting transfers between devices: 30.8 us -> none  [the longest x1 8.42 us: shards(): lax.all_to_all(cut_input, 'ep', split_axis=0, concat_axis=0, tiled=True)]
    all_to_all x2 -> x0, blocking collectives: 25.6 us -> none  [the longest x1 16.6 us: shards(): lax.all_to_all(cut_cotan, 'ep', split_axis=0, concat_axis=0, tiled=True)]
    unnamed x1 -> x0, blocking collectives: 23.5 us -> none
    all_to_all x5 -> x0, waiting for transfers between devices: 21.3 us -> none  [the longest x1 14.4 us: summed_on_arrival(): tiles = lax.all_to_all(cut_along(array, dim, peers), axis, 0, 0, tiled=True)]
  transfers between devices with their start and end apart: 7 -> 0, of which waited for: 4 -> 0; matrix products, arithmetic and copies ran while one was open for 23% -> 0% of each run, Pallas kernels for 0% -> 0%
where the time goes in v2:
time: 128 us; the launch traced here: 127 us
  Pallas kernels  115 us (90%)
  other arithmetic  4.05 us (3%)
  matrix products  3.88 us (3%)
  local copies, waits for them, and re-layouts  2.89 us (2%)
    pallas_call x1, Pallas kernels, exchange(): pl.pallas_call(functools.partial(exchange_kernel, n), out_shape=(jax.Shap...  101 us
    pallas_call x1, Pallas kernels, gradients(): pl.pallas_call(gradient_kernel, grid=(experts, model // chunk), out_shape...  14 us
    dot_general x1, matrix products, shards(): rows = jnp.dot(pick_rows, source, preferred_element_type=F32).astype(BF)  3.73 us

profile of v2, /device:TPU:1, one launch (start us, length us, event | category | flops | bytes accessed | tf_op | source)
XLA Modules:
  0.0 126.9 jit_solution(13175086074234692116)
XLA Ops:
  0.6 0.0 copy-start
  0.7 0.8 convert_bitcast_fusion
  1.5 0.1 eq.47
  1.5 0.7 select_reduce_fusion.1
  2.3 0.1 convolution_select_fusion
  2.4 0.4 fusion
  2.8 0.6 pad.4.weight_ref
  3.4 1.2 fusion.8
  4.6 0.0 copy-done
  4.6 3.7 %convolution_convert_fusion = bf16[1536,1024]{1,0:T(8,128)(2,1)} fusion(pred[1536,256]{1,0:T(32,128)(4,1)S(1)} %get-tuple-element.25, bf16[256,2048]{1,0:T(8,128)(2,1)S(1)} %copy-done, s32[]{:T(128)S(6)} %select_n.40, bf16[256,2048]{1,0:T(8,128)(2,1)} %tok_ref.1, pred[]{:T(512)S(6)} %eq.50), kind=kOutput, calls=%fused_computation | convolution fusion | flops 807141376 | bytes 4587525 | tf_op jit(solution)/shard_map/dot_general | solution.py:524
  8.4 0.0 copy-start.3
  8.4 101.4 %shard_map.136 = (bf16[2,2,16,48,2048]{4,3,2,1,0:T(8,128)(2,1)}, bf16[3,4,384,256]{3,2,1,0:T(8,128)(2,1)}, bf16[256,256]{1,0:T(8,128)(2,1)}, f32[16,8,128]{2,1,0:T(8,128)}, f32[256,128]{1,0:T(8,128)}) custom-call(bf16[16,2,48,1024]{3,2,1,0:T(8,128)(2,1)} %bitcast.18, f32[16,8,128]{2,1,0:T(8,128)} %pad.4.weight_ref, bf16[2,2048,256]{2,1,0:T(8,128)(2,1)} %wg_ref.1, ...), custom_call_target="tpu_custom_call" | custom-call | tf_op jit(solution)/shard_map/pallas_call | solution.py:414
  109.8 0.8 slice.3
  110.6 0.4 fusion.1
  111.0 0.0 copy-done.3
  111.0 0.6 select_reduce_fusion
  111.6 0.0 copy-start.2
  111.6 0.0 copy-start.1
  111.6 14.0 %shard_map.137 = (f32[2,2048,256]{2,1,0:T(8,128)}, f32[2,2048,256]{2,1,0:T(8,128)}, f32[2,256,2048]{2,1,0:T(8,128)}) custom-call(bf16[2,2,768,2048]{3,2,1,0:T(8,128)(2,1)} %bitcast.16, bf16[2,2,768,2048]{3,2,1,0:T(8,128)(2,1)} %bitcast.17, bf16[3,4,384,256]{3,2,1,0:T(8,128)(2,1)} %get-tuple-element.17.act_ref), custom_call_target="tpu_custom_call" | custom-call | tf_op jit(solution)/shard_map/pallas_call | solution.py:471
  125.6 0.0 copy-done.2
  125.6 0.7 copy.19
  126.2 0.0 copy-done.1
  126.2 0.7 copy.20
  (2 shorter events, 0.0 us)
Async XLA Ops:
  0.6 4.0 %copy-start = (bf16[256,2048]{1,0:T(8,128)(2,1)S(1)}, bf16[256,2048]{1,0:T(8,128)(2,1)}, u32[]{:S(2)}) copy-start(bf16[256,2048]{1,0:T(8,128)(2,1)} %cot_ref.1) | copy-start | bytes 3145732
  8.4 102.6 %copy-start.3 = (s32[256,4]{0,1:T(4,128)S(1)}, s32[256,4]{0,1:T(4,128)}, u32[]{:S(2)}) copy-start(s32[256,4]{0,1:T(4,128)} %param.11) | copy-start | bytes 12292
  111.6 14.0 %copy-start.2 = (bf16[256,256]{1,0:T(8,128)(2,1)S(1)}, bf16[256,256]{1,0:T(8,128)(2,1)}, u32[]{:S(2)}) copy-start(bf16[256,256]{1,0:T(8,128)(2,1)} %get-tuple-element.32) | copy-start | bytes 393220
  111.6 14.7 %copy-start.1 = (f32[256,128]{1,0:T(8,128)S(1)}, f32[256,128]{1,0:T(8,128)}, u32[]{:S(2)}) copy-start(f32[256,128]{1,0:T(8,128)} %get-tuple-element.37) | copy-start | bytes 393220

commit v3 on v2

--- a/solution.py
+++ b/solution.py
@@ -17,8 +17,9 @@
     (0, 0), (0, 1), (1, 0), (0, 3), (3, 0), (1, 1), (3, 3), (1, 3),
     (3, 1), (0, 2), (2, 0), (2, 2), (1, 2), (2, 1), (3, 2), (2, 3),
 )
-GROUP = 8
-LAG = 3
+GROUP = 4
+LAG = 5
+SLACK = 3
 
 
 def place():
@@ -39,10 +40,8 @@
 
 
 def greet(devices):
-    barrier = pltpu.get_barrier_semaphore()
     for device in devices:
-        pl.semaphore_signal(barrier, inc=1, device_id=device, device_id_type=MESH)
-    pl.semaphore_wait(barrier, len(devices))
+        pl.semaphore_signal(pltpu.get_barrier_semaphore(), inc=1, device_id=device, device_id_type=MESH)
 
 
 def remote(src, dst, send, recv, device):
@@ -64,16 +63,18 @@
 
 
 def exchange_kernel(
-    n, rows_ref, weight_ref, wg_ref, wu_ref, wd_ref, tok_ref, cot_ref, scale_ref, dw_ref, pick_ref,
-    held_ref, act_out, token_ref, home_score, dense_out,
-    r, rw, wg, wu, wd, act, back, mine, part, first, second, total, home, score, scores, to_home,
+    n, slots, weight_ref, wg_ref, wu_ref, wd_ref, tok_ref, cot_ref, scale_ref, dw_ref, pick_ref,
+    gate_out, up_out, down_out, token_ref, home_score, dense_out,
+    sent, source, gate_sum, up_sum, down_sum, r, rw, wg, wu, wd, act, back, mine, part, first, second, total, home, score, scores, to_home,
     tok, cot, pick, dsend, dland, dwall,
     a_send, a_recv, w_send, w_recv, b_send, b_recv, g_send, g_recv,
     y_send, y_recv, o_send, o_recv, q_send, q_recv, d_send, d_recv, f_send, f_recv, h_send, h_recv,
     t_send, t_recv, s_send, s_recv, k_send, k_recv, load, local, out_sem,
 ):
     ep, tp, y, c = place()
-    slots, half = rows_ref.shape[2:]
+    half = cot_ref.shape[1] // 2
+    per = n // GROUP
+    groups = 2 * per
     quarter, block, width = half // 2, half // 4, dw_ref.shape[1]
     rows = GROUP * slots
     par = lax.rem(y, 2)
@@ -88,8 +89,22 @@
     mine_cols = columns(c * half, half)
     ep_cols = columns(ep * width, width)
 
+    greet([(targets[i], tp) for i in range(1, n)] + others)
+    pick_load = pltpu.make_async_copy(pick_ref, pick, load.at[0])
+    pick_load.start()
+    token_part = pltpu.make_async_copy(tok_ref.at[:, mine_cols], source, load.at[1])
+    cotan_part = pltpu.make_async_copy(cot_ref.at[:, mine_cols], source, load.at[1])
+
+    @pl.when(par == 0)
+    def _():
+        token_part.start()
+
+    @pl.when(par == 1)
+    def _():
+        cotan_part.start()
+
     loads = [
-        pltpu.make_async_copy(a, b, load.at[k])
+        pltpu.make_async_copy(a, b, load.at[2 + k])
         for k, (a, b) in enumerate(
             [
                 (tok_ref.at[:, columns(tp * block, block)], tok),
@@ -97,21 +112,31 @@
                 (wg_ref, wg),
                 (wu_ref, wu),
                 (wd_ref, wd),
-                (pick_ref, pick),
                 (dw_ref, dwall.at[:, ep_cols]),
                 (weight_ref.at[ep], rw.at[0]),
-                (rows_ref.at[ep, 0], r.at[par, 0, 0, :, mine_cols]),
-                (rows_ref.at[ep, 1], r.at[par, 1, 0, :, mine_cols]),
             ]
         )
     ]
     for copy in loads:
         copy.start()
-    greet([(targets[i], tp) for i in range(1, n)] + others + [up, down])
+    pick_load.wait()
+    token_part.wait()
+    few = n // SIDE
+    for k in range(SIDE):
+        for m in range(2):
+            cols = pl.ds(m * quarter, quarter)
+            chosen = nn(pick[k * few * 2 * slots : (k + 1) * few * 2 * slots], source[:, cols])
+            sent[k * few : (k + 1) * few, :, :, cols] = chosen.astype(BF).reshape(few, 2, slots, quarter)
+    own_rows = [
+        pltpu.make_async_copy(sent.at[ep, e], r.at[par, e, 0, :, mine_cols], load.at[9 + e]) for e in range(2)
+    ]
+    for copy in own_rows:
+        copy.start()
+    pl.semaphore_wait(pltpu.get_barrier_semaphore(), n - 1 + len(others))
 
     def a_copy(e, i, to):
         return remote(
-            rows_ref.at[to, e], r.at[par, e, i, :, mine_cols], a_send.at[e, i], a_recv.at[e, i], (to, tp)
+            sent.at[to, e], r.at[par, e, i, :, mine_cols], a_send.at[e, i], a_recv.at[e, i], (to, tp)
         )
 
     def w_copy(i):
@@ -143,7 +168,7 @@
     dland[0] = dsend[:, ep_cols]
     for i in range(1, n):
         g_copy(i).start()
-    for copy in loads[2:]:
+    for copy in loads[2:] + own_rows:
         copy.wait()
     for i in range(1, n):
         w_copy(i).wait_recv()
@@ -181,14 +206,14 @@
                 q_copy(e, i, way).start()
 
     def group(q):
-        return q // 2, pl.ds(lax.rem(q, 2) * GROUP, GROUP)
+        return q // per, pl.ds(lax.rem(q, per) * GROUP, GROUP)
 
     def ready(q):
-        e = q // 2
+        e = q // per
 
         @pl.loop(0, GROUP)
         def _(k):
-            i = lax.rem(q, 2) * GROUP + k
+            i = lax.rem(q, per) * GROUP + k
             o_copy(e, i).wait_recv()
             for way in range(2):
                 q_copy(e, i, way).wait_recv()
@@ -210,9 +235,7 @@
         swish = gate_val * squash
         hidden = ((up_val + 1.0) * swish).astype(BF).astype(F32)
         row_score = jnp.sum(hidden * down_back, axis=1, keepdims=True).reshape(GROUP, slots, 1)
-        score[pl.ds(pl.multiple_of(q * GROUP, GROUP), GROUP), :] = jnp.sum(
-            jnp.where(diagonal[None], row_score, 0.0), axis=1
-        )
+        score[q] = jnp.sum(jnp.where(diagonal[None], row_score, 0.0), axis=1)
         hidden_back = weight * down_back
         slope = squash + sigmoid_slope * swish * (1.0 - squash)
         act[0, q] = (weight * hidden).astype(BF)
@@ -244,13 +267,12 @@
         )
 
     def t_copy(q, k, to):
-        i = lax.rem(q, 2) * GROUP + k
         return remote(
-            total.at[q, pl.ds(k * slots, slots)], home.at[ep, q // 2], t_send.at[q, k], t_recv.at[q, k], (to, tp)
+            total.at[q, pl.ds(k * slots, slots)], home.at[ep, q // per], t_send.at[q, k], t_recv.at[q, k], (to, tp)
         )
 
     def own_total(e):
-        return pltpu.make_async_copy(total.at[2 * e, pl.ds(0, slots)], home.at[ep, e], local.at[e])
+        return pltpu.make_async_copy(total.at[per * e, pl.ds(0, slots)], home.at[ep, e], local.at[e])
 
     def core_sum(q):
         for j in range(4):
@@ -278,25 +300,35 @@
         value = part[q, :, columns(y * block, block)].astype(F32)
         total[q] = (value + second[0, q].astype(F32) + second[1, q].astype(F32)).astype(BF)
         for k in range(GROUP):
-            to = jnp.where(lax.rem(q, 2) == 0, homes[k], homes[GROUP + k])
+            to = homes[k]
+            for m in range(1, per):
+                to = jnp.where(lax.rem(q, per) == m, homes[m * GROUP + k], to)
             if k == 0:
 
-                @pl.when(lax.rem(q, 2) == 0)
+                @pl.when(lax.rem(q, per) == 0)
                 def _():
-                    own_total(q // 2).start()
-
-                @pl.when(lax.rem(q, 2) == 1)
-                def _():
-                    t_copy(q, 0, homes[GROUP]).start()
+                    own_total(q // per).start()
+
+                @pl.when(lax.rem(q, per) > 0)
+                def _(to=to):
+                    t_copy(q, 0, to).start()
 
             else:
                 t_copy(q, k, to).start()
 
-    def held_copy(a, e):
-        return pltpu.make_async_copy(r.at[a, e], held_ref.at[a, e], out_sem.at[a, e])
-
-    def act_copy(q):
-        return pltpu.make_async_copy(act.at[:, q], act_out.at[:, q], out_sem.at[2, q])
+    def sum_chunk(e, k):
+        cols = pl.ds(pl.multiple_of(k * quarter, quarter), quarter)
+        of_expert = pl.ds(e * per, per)
+        x = r[0, e, :, :, cols].reshape(n * slots, quarter)
+        cotan = r[1, e, :, :, cols].reshape(n * slots, quarter)
+        hidden, gate_back, up_back = (act[a, of_expert].reshape(n * slots, act.shape[3]) for a in range(3))
+        gate_sum[e, cols, :] = tn(x, gate_back).astype(BF)
+        up_sum[e, cols, :] = tn(x, up_back).astype(BF)
+        down_sum[e, :, cols] = tn(hidden, cotan).astype(BF)
+
+    def sum_copies(e):
+        pairs = [(gate_sum, gate_out), (up_sum, up_out), (down_sum, down_out)]
+        return [pltpu.make_async_copy(a.at[e], b.at[e], out_sem.at[e, k]) for k, (a, b) in enumerate(pairs)]
 
     def score_copy(k):
         return remote(score, scores.at[tp], s_send.at[k], s_recv.at[k], (ep, lax.rem(tp + k, 8)))
@@ -304,18 +336,18 @@
     def k_copy(i):
         return remote(to_home.at[i], home_score.at[ep], k_send.at[i], k_recv.at[i], (homes[i], tp))
 
-    @pl.loop(0, 7)
+    @pl.loop(0, groups + 3)
     def _(q):
-        start = jnp.where(q == 0, 0, jnp.minimum(q * GROUP + 2 * LAG, 2 * n + LAG))
-        stop = jnp.where(q >= 3, 2 * n + LAG, (q + 1) * GROUP + 2 * LAG)
-        start = jnp.where(q >= 4, 2 * n + LAG, start)
+        last = 2 * n + LAG
+        start = jnp.where(q == 0, 0, jnp.where(q >= groups, last, jnp.minimum(q * GROUP + LAG + SLACK, last)))
+        stop = jnp.where(q >= groups - 1, last, jnp.minimum((q + 1) * GROUP + LAG + SLACK, last))
         pl.loop(start, stop)(serve)
 
-        @pl.when((q >= 1) & (q < 5))
+        @pl.when((q >= 1) & (q < groups + 1))
         def _():
             core_sum(q - 1)
 
-        @pl.when((q >= 2) & (q < 6))
+        @pl.when((q >= 2) & (q < groups + 2))
         def _():
             ring_sum(q - 2)
 
@@ -323,27 +355,34 @@
         def _():
             home_sum(q - 3)
 
-        @pl.when(q < 4)
+        @pl.when(q < groups)
         def _():
             ready(q)
             expert_rows(q)
             for j in range(4):
                 d_copy(q, j).start()
-            act_copy(q).start()
-
-            @pl.when(lax.rem(q, 2) == 1)
-            def _():
-                held_copy(0, q // 2).start()
-                held_copy(1, q // 2).start()
-
-        @pl.when(q == 3)
-        def _():
+
+        @pl.when((q >= per) & (q < groups + 2))
+        def _():
+            chunk = jnp.where(q < groups, q - per, 2 * (q - groups))
+            chunk_stop = jnp.where(q < groups, chunk + 1, chunk + 2)
+
+            @pl.loop(chunk, chunk_stop)
+            def _(k):
+                sum_chunk(jnp.where(q < groups, 0, 1), k)
+
+        @pl.when(q == groups - 1)
+        def _():
+            for copy in sum_copies(0):
+                copy.start()
             for k in range(1, 8):
                 score_copy(k).start()
             scores[tp] = score[...]
 
-        @pl.when(q == 4)
-        def _():
+        @pl.when(q == groups + 1)
+        def _():
+            for copy in sum_copies(1):
+                copy.start()
             for k in range(1, 8):
                 score_copy(k).wait_recv()
             every = scores[0]
@@ -351,7 +390,8 @@
                 every = every + scores[k]
             lower = lax.broadcasted_iota(jnp.int32, (8, 128), 0) == 0
             for i in range(n):
-                to_home[i] = jnp.where(lower, every[i : i + 1, :], every[n + i : n + i + 1, :])
+                g, k = i // GROUP, i % GROUP
+                to_home[i] = jnp.where(lower, every[g, k : k + 1, :], every[per + g, k : k + 1, :])
             pltpu.make_async_copy(to_home.at[0], home_score.at[ep], local.at[2]).start()
             for i in range(1, n):
                 k_copy(i).start()
@@ -365,16 +405,6 @@
     dense_out[...] = dense
     back_dense = nt(cot[...], dwall[...])
 
-    own_total(0).wait()
-    own_total(1).wait()
-    for q in range(4):
-        for k in range(GROUP):
-            if k > 0 or q % 2 == 1:
-                t_copy(q, k, homes[1]).wait_recv()
-    got = tn(pick[...], home[...].reshape(n * 2 * slots, block))
-    token_ref[...] = (got + back_dense).astype(BF)
-
-    pltpu.make_async_copy(to_home.at[0], home_score.at[ep], local.at[2]).wait()
     for e in range(2):
         for i in range(n):
             if i > 0:
@@ -385,59 +415,77 @@
                 q_copy(e, i, way).wait_send()
     for i in range(1, n):
         w_copy(i).wait_send()
-        k_copy(i).wait()
     for k in range(1, 8):
         score_copy(k).wait_send()
-    for q in range(4):
-        act_copy(q).wait()
+    for q in range(groups):
         for j in range(4):
             d_copy(q, j).wait_send()
         for way in range(2):
             f_copy(q, way).wait_send()
             h_copy(q, way).wait_send()
+    own_total(0).wait()
+    own_total(1).wait()
+    for q in range(groups):
         for k in range(GROUP):
-            if k > 0 or q % 2 == 1:
+            if k > 0 or q % per > 0:
+                t_copy(q, k, homes[1]).wait_recv()
+    got = tn(pick[...], home[...].reshape(n * 2 * slots, block))
+    token_ref[...] = (got + back_dense).astype(BF)
+
+    pltpu.make_async_copy(to_home.at[0], home_score.at[ep], local.at[2]).wait()
+    for i in range(1, n):
+        k_copy(i).wait()
+    for q in range(groups):
+        for k in range(GROUP):
+            if k > 0 or q % per > 0:
                 t_copy(q, k, homes[1]).wait_send()
     for e in range(2):
-        held_copy(0, e).wait()
-        held_copy(1, e).wait()
-
-
-def exchange(rows, weights, wg, wu, wd, tokens, cotangent, scale, dw, pick):
-    n, _, slots, half = rows.shape
-    model, block, width = 2 * half, half // 4, dw.shape[1]
-    tok_rows = tokens.shape[0]
+        for copy in sum_copies(e):
+            copy.wait()
+
+
+def exchange(weights, wg, wu, wd, tokens, cotangent, scale, dw, pick):
+    n = weights.shape[0]
+    slots = pick.shape[0] // (2 * n)
+    tok_rows, model = tokens.shape
+    half, block, width = model // 2, model // 8, dw.shape[1]
     units = wg.shape[2]
     dma, vmem = pltpu.SemaphoreType.DMA, pltpu.VMEM
-    many = GROUP * slots
+    many, groups = GROUP * slots, 2 * n // GROUP
     any_space, in_vmem = pl.BlockSpec(memory_space=pl.ANY), pl.BlockSpec(memory_space=vmem)
     return pl.pallas_call(
-        functools.partial(exchange_kernel, n),
+        functools.partial(exchange_kernel, n, slots),
         out_shape=(
-            jax.ShapeDtypeStruct((2, 2, n, slots, model), BF),
-            jax.ShapeDtypeStruct((3, 4, many, units), BF),
+            jax.ShapeDtypeStruct(wg.shape, BF),
+            jax.ShapeDtypeStruct(wu.shape, BF),
+            jax.ShapeDtypeStruct(wd.shape, BF),
             jax.ShapeDtypeStruct((tok_rows, block), BF),
             jax.ShapeDtypeStruct(weights.shape, F32),
             jax.ShapeDtypeStruct((block, width), F32),
         ),
-        in_specs=[any_space] * 7 + [in_vmem] + [any_space] * 2,
-        out_specs=[any_space, any_space, in_vmem, any_space, in_vmem],
+        in_specs=[any_space] * 6 + [in_vmem] + [any_space] * 2,
+        out_specs=[any_space, any_space, any_space, in_vmem, any_space, in_vmem],
         scratch_shapes=[
+            vmem((n, 2, slots, half), BF),
+            vmem((tok_rows, half), BF),
+            vmem(wg.shape, BF),
+            vmem(wu.shape, BF),
+            vmem(wd.shape, BF),
             vmem((2, 2, n, slots, model), BF),
             vmem(weights.shape, F32),
             vmem(wg.shape, BF),
             vmem(wu.shape, BF),
             vmem(wd.shape, BF),
-            vmem((3, 4, many, units), BF),
-            vmem((4, many, model), BF),
-            vmem((4, many, half), BF),
-            vmem((4, many, half), BF),
-            vmem((2, 4, many, block // 2), BF),
-            vmem((2, 4, many, block), BF),
-            vmem((4, many, block), BF),
+            vmem((3, groups, many, units), BF),
+            vmem((groups, many, model), BF),
+            vmem((groups, many, half), BF),
+            vmem((groups, many, half), BF),
+            vmem((2, groups, many, block // 2), BF),
+            vmem((2, groups, many, block), BF),
+            vmem((groups, many, block), BF),
             vmem((n, 2, slots, block), BF),
-            vmem((2 * n, 128), F32),
-            vmem((8, 2 * n, 128), F32),
+            vmem((groups, GROUP, 128), F32),
+            vmem((8, groups, GROUP, 128), F32),
             vmem(weights.shape, F32),
             vmem((tok_rows, block), BF),
             vmem(cotangent.shape, BF),
@@ -447,46 +495,12 @@
             vmem((block, model), BF),
             dma((2, n)), dma((2, n)), dma((n,)), dma((n,)), dma((n,)), dma((n,)), dma((n,)), dma((n,)),
             dma((2, 2, n)), dma((2, 2, n)), dma((2, n)), dma((2, n)), dma((2, 2, n)), dma((2, 2, n)),
-            dma((4, 4)), dma((4, 4)), dma((2, 4)), dma((2, 4)), dma((2, 4)), dma((2, 4)),
-            dma((4, GROUP)), dma((4, GROUP)), dma((8,)), dma((8,)), dma((n,)), dma((n,)),
-            dma((10,)), dma((3,)), dma((3, 4)),
+            dma((4, groups)), dma((4, groups)), dma((2, groups)), dma((2, groups)), dma((2, groups)), dma((2, groups)),
+            dma((groups, GROUP)), dma((groups, GROUP)), dma((8,)), dma((8,)), dma((n,)), dma((n,)),
+            dma((11,)), dma((3,)), dma((2, 3)),
         ],
-        compiler_params=pltpu.CompilerParams(collective_id=0, has_side_effects=True, vmem_limit_bytes=62 << 20),
-    )(rows, weights, wg, wu, wd, tokens, cotangent, scale, dw, pick)
-
-
-def gradient_kernel(x_ref, c_ref, act_ref, gate_ref, up_ref, down_ref):
-    x, cotan = x_ref[0, 0], c_ref[0, 0]
-    many = act_ref.shape[2] * act_ref.shape[1]
-    hidden, gate_back, up_back = (act_ref[k].reshape(many, act_ref.shape[3]) for k in range(3))
-    gate_ref[0] = tn(x, gate_back)
-    up_ref[0] = tn(x, up_back)
-    down_ref[0] = tn(hidden, cotan)
-
-
-def gradients(held, act):
-    _, experts, many, model = held.shape
-    units = act.shape[3]
-    chunk = model // 4
-    return pl.pallas_call(
-        gradient_kernel,
-        grid=(experts, model // chunk),
-        out_shape=(
-            jax.ShapeDtypeStruct((experts, model, units), F32),
-            jax.ShapeDtypeStruct((experts, model, units), F32),
-            jax.ShapeDtypeStruct((experts, units, model), F32),
-        ),
-        in_specs=[
-            pl.BlockSpec((1, 1, many, chunk), lambda e, k: (0, e, 0, k)),
-            pl.BlockSpec((1, 1, many, chunk), lambda e, k: (1, e, 0, k)),
-            pl.BlockSpec((3, 2, many // 2, units), lambda e, k: (0, e, 0, 0)),
-        ],
-        out_specs=[
-            pl.BlockSpec((1, chunk, units), lambda e, k: (e, k, 0)),
-            pl.BlockSpec((1, chunk, units), lambda e, k: (e, k, 0)),
-            pl.BlockSpec((1, units, chunk), lambda e, k: (e, 0, k)),
-        ],
-    )(held, held, act)
+        compiler_params=pltpu.CompilerParams(collective_id=0, has_side_effects=True, vmem_limit_bytes=63 << 20),
+    )(weights, wg, wu, wd, tokens, cotangent, scale, dw, pick)
 
 
 def shards(
@@ -498,9 +512,6 @@
     n = lax.axis_size("ep")
     experts = local_count * n
     slots = tok_rows * top_count * 3 // (2 * experts)
-    half, block = model // 2, model // 8
-    ep, tp, y, c = place()
-
     names = expert_ids.T[None] == jnp.arange(experts, dtype=jnp.int32)[:, None, None]
     member = jnp.sum(names.astype(F32), axis=1)
     weight_of = jnp.sum(jnp.where(names, route_weights.T[None].astype(F32), 0.0), axis=1)
@@ -516,24 +527,22 @@
     pick_rows = pick.reshape(experts * slots, tok_rows)
     weights = jnp.pad(slot_weight.reshape(n, local_count, slots), ((0, 0), (0, 8 - local_count), (0, 128 - slots)))
 
-    source = jnp.where(
-        lax.rem(y, 2) == 0,
-        lax.dynamic_slice_in_dim(tokens, c * half, half, 1),
-        lax.dynamic_slice_in_dim(cotangent, c * half, half, 1),
+    grad_gate, grad_up, grad_down, token_grad, home_score, dense_grad = exchange(
+        weights, gate_weight, up_weight, down_weight, tokens, cotangent, dense_gate[None, :], dense_weight, pick_rows
     )
-    rows = jnp.dot(pick_rows, source, preferred_element_type=F32).astype(BF)
-    rows = rows.reshape(n, local_count, slots, half)
-
-    held, act, token_grad, home_score, dense_grad = exchange(
-        rows, weights, gate_weight, up_weight, down_weight, tokens, cotangent, dense_gate[None, :], dense_weight, pick_rows
-    )
-    grad_gate, grad_up, grad_down = gradients(held.reshape(2, local_count, n * slots, model), act)
 
     slot_score = home_score[:, :local_count, :slots].reshape(experts, slots, 1)
     of_expert = jnp.sum(jnp.where(picked, slot_score, 0.0), axis=1)
     of_choice = jnp.sum(jnp.where(names, of_expert[:, None, :], 0.0), axis=0)
     weight_grad = of_choice.T.astype(BF)
-    return token_grad, weight_grad, grad_gate, grad_up, grad_down, dense_grad
+    return (
+        token_grad,
+        weight_grad,
+        grad_gate.astype(F32),
+        grad_up.astype(F32),
+        grad_down.astype(F32),
+        dense_grad,
+    )
 
 
 def solution(mesh):

time: 128 us -> 118 us (0.922)
  Pallas kernels: 115 us -> 100 us
  other arithmetic: 4.05 us -> 12.9 us
  matrix products: 3.88 us -> 0.15 us
    pallas_call x2 -> x1, Pallas kernels: 115 us -> 100 us  [exchange(): pl.pallas_call(functools.partial(exchange_kernel, n, slots), out_shape=(j...]
    convert_element_type x0 -> x3, other arithmetic: none -> 8.97 us  [the longest x1 4.08 us: shards(): grad_gate.astype(F32)]
    dot_general x1 -> x0, matrix products: 3.73 us -> none  [shards(): rows = jnp.dot(pick_rows, source, preferred_element_type=F32).astype(BF)]
where the time goes in v3:
time: 118 us; the launch traced here: 117 us
  Pallas kernels  100 us (85%)
  other arithmetic  12.9 us (11%)
  local copies, waits for them, and re-layouts  2.89 us (2%)
    pallas_call x1, Pallas kernels, exchange(): pl.pallas_call(functools.partial(exchange_kernel, n, slots), out_shape=(j...  100 us
    convert_element_type x1, other arithmetic, shards(): grad_gate.astype(F32)  4.08 us
    convert_element_type x1, other arithmetic, shards(): grad_down.astype(F32)  2.54 us

profile of v3, /device:TPU:1, one launch (start us, length us, event | category | flops | bytes accessed | tf_op | source)
XLA Modules:
  0.0 117.0 jit_solution(16069612417358143649)
XLA Ops:
  0.6 0.7 convert_bitcast_fusion
  1.3 0.1 eq.45
  1.4 0.7 convert_reduce_fusion
  2.1 0.1 convolution_select_fusion
  2.3 0.4 fusion
  2.6 0.6 pad.4.weight_ref
  3.3 1.1 fusion.2.pick_ref
  4.4 0.0 copy-start.4
  4.4 100.4 %shard_map.136 = (bf16[2,2048,256]{2,1,0:T(8,128)(2,1)}, bf16[2,2048,256]{2,1,0:T(8,128)(2,1)}, bf16[2,256,2048]{2,1,0:T(8,128)(2,1)}, bf16[256,256]{1,0:T(8,128...) custom-call(f32[16,8,128]{2,1,0:T(8,128)} %pad.4.weight_ref, bf16[2,2048,256]{2,1,0:T(8,128)(2,1)} %wg_ref.1, ...), custom_call_target="tpu_custom_call" | custom-call | tf_op jit(solution)/shard_map/pallas_call | solution.py:456
  104.9 0.8 slice.3
  105.7 0.4 fusion.1
  106.1 0.0 copy-done.4
  106.1 0.6 select_reduce_fusion
  106.7 0.0 copy-start.1
  106.7 4.1 %convert_element_type.52 = f32[2,2048,256]{2,1,0:T(8,128)} convert(bf16[2,2048,256]{2,1,0:T(8,128)(2,1)} %get-tuple-element.14) | non-fusion elementwise | flops 1048576 | bytes 6291456 | tf_op jit(solution)/shard_map/convert_element_type | solution.py:541
  110.8 0.0 copy-done.1
  110.8 0.0 copy-start
  110.8 2.3 %convert_element_type.53 = f32[2,2048,256]{2,1,0:T(8,128)} convert(bf16[2,2048,256]{2,1,0:T(8,128)(2,1)S(1)} %copy-done.1) | non-fusion elementwise | flops 1048576 | bytes 6291456 | tf_op jit(solution)/shard_map/convert_element_type | solution.py:542
  113.2 0.0 copy-done
  113.2 0.0 copy-start.3
  113.2 0.0 copy-start.2
  113.2 2.5 %convert_element_type.54 = f32[2,256,2048]{2,1,0:T(8,128)} convert(bf16[2,256,2048]{2,1,0:T(8,128)(2,1)S(1)} %copy-done) | non-fusion elementwise | flops 1048576 | bytes 6291456 | tf_op jit(solution)/shard_map/convert_element_type | solution.py:543
  115.7 0.0 copy-done.3
  115.7 0.7 copy.17
  116.4 0.0 copy-done.2
  116.4 0.7 copy.18
  (2 shorter events, 0.0 us)
Async XLA Ops:
  4.4 101.7 %copy-start.4 = (s32[256,4]{0,1:T(4,128)S(1)}, s32[256,4]{0,1:T(4,128)}, u32[]{:S(2)}) copy-start(s32[256,4]{0,1:T(4,128)} %param.11) | copy-start | bytes 12292
  106.7 4.1 %copy-start.1 = (bf16[2,2048,256]{2,1,0:T(8,128)(2,1)S(1)}, bf16[2,2048,256]{2,1,0:T(8,128)(2,1)}, u32[]{:S(2)}) copy-start(bf16[2,2048,256]{2,1,0:T(8,128)(2,1)} %get-tuple-element.15) | copy-start | bytes 6291460
  110.8 2.3 %copy-start = (bf16[2,256,2048]{2,1,0:T(8,128)(2,1)S(1)}, bf16[2,256,2048]{2,1,0:T(8,128)(2,1)}, u32[]{:S(2)}) copy-start(bf16[2,256,2048]{2,1,0:T(8,128)(2,1)} %get-tuple-element.16) | copy-start | bytes 6291460
  113.2 2.5 %copy-start.3 = (bf16[256,256]{1,0:T(8,128)(2,1)S(1)}, bf16[256,256]{1,0:T(8,128)(2,1)}, u32[]{:S(2)}) copy-start(bf16[256,256]{1,0:T(8,128)(2,1)} %get-tuple-element.26) | copy-start | bytes 393220
  113.2 3.2 %copy-start.2 = (f32[256,128]{1,0:T(8,128)S(1)}, f32[256,128]{1,0:T(8,128)}, u32[]{:S(2)}) copy-start(f32[256,128]{1,0:T(8,128)} %get-tuple-element.31) | copy-start | bytes 393220

commit v4 on v3

--- a/solution.py
+++ b/solution.py
@@ -336,7 +336,7 @@
     def k_copy(i):
         return remote(to_home.at[i], home_score.at[ep], k_send.at[i], k_recv.at[i], (homes[i], tp))
 
-    @pl.loop(0, groups + 3)
+    @pl.loop(0, groups + 5)
     def _(q):
         last = 2 * n + LAG
         start = jnp.where(q == 0, 0, jnp.where(q >= groups, last, jnp.minimum(q * GROUP + LAG + SLACK, last)))
@@ -347,13 +347,13 @@
         def _():
             core_sum(q - 1)
 
-        @pl.when((q >= 2) & (q < groups + 2))
-        def _():
-            ring_sum(q - 2)
-
-        @pl.when(q >= 3)
-        def _():
-            home_sum(q - 3)
+        @pl.when((q >= 3) & (q < groups + 3))
+        def _():
+            ring_sum(q - 3)
+
+        @pl.when(q >= 5)
+        def _():
+            home_sum(q - 5)
 
         @pl.when(q < groups)
         def _():

time: 118 us -> 114 us (0.966)
  Pallas kernels: 100 us -> 96.6 us
    pallas_call x1, Pallas kernels: 100 us -> 96.6 us  [exchange(): pl.pallas_call(functools.partial(exchange_kernel, n, slots), out_shape=(j...]
where the time goes in v4:
time: 114 us; the launch traced here: 113 us
  Pallas kernels  96.6 us (85%)
  other arithmetic  12.9 us (11%)
  local copies, waits for them, and re-layouts  2.89 us (3%)
    pallas_call x1, Pallas kernels, exchange(): pl.pallas_call(functools.partial(exchange_kernel, n, slots), out_shape=(j...  96.6 us
    convert_element_type x1, other arithmetic, shards(): grad_gate.astype(F32)  4.08 us
    convert_element_type x1, other arithmetic, shards(): grad_down.astype(F32)  2.54 us
    convert_element_type x1, other arithmetic, shards(): grad_up.astype(F32)  2.34 us

profile of v4, /device:TPU:1, one launch (start us, length us, event | category | flops | bytes accessed | tf_op | source)
XLA Modules:
  0.0 113.2 jit_solution(6998290442928220335)
XLA Ops:
  0.6 0.7 convert_bitcast_fusion
  1.3 0.1 eq.45
  1.4 0.7 convert_reduce_fusion
  2.1 0.1 convolution_select_fusion
  2.3 0.4 fusion
  2.6 0.6 pad.4.weight_ref
  3.3 1.1 %fusion.2.pick_ref = bf16[1536,256]{1,0:T(8,128)(2,1)} fusion(f32[1536]{0:T(1024)S(1)} %eq.45, f32[32,256]{1,0:T(8,128)S(1)} %convolution_select_fusion), kind=kLoop, calls=%fused_computation.5 | loop fusion | flops 786432 | bytes 825344 | tf_op jit(solution)/shard_map/convert_element_type | solution.py:525
  4.4 0.0 copy-start.4
  4.4 96.6 %shard_map.136 = (bf16[2,2048,256]{2,1,0:T(8,128)(2,1)}, bf16[2,2048,256]{2,1,0:T(8,128)(2,1)}, bf16[2,256,2048]{2,1,0:T(8,128)(2,1)}, bf16[256,256]{1,0:T(8,128...) custom-call(f32[16,8,128]{2,1,0:T(8,128)} %pad.4.weight_ref, bf16[2,2048,256]{2,1,0:T(8,128)(2,1)} %wg_ref.1, ...), custom_call_target="tpu_custom_call" | custom-call | tf_op jit(solution)/shard_map/pallas_call | solution.py:456
  101.1 0.8 slice.3
  101.9 0.4 fusion.1
  102.3 0.0 copy-done.4
  102.3 0.6 select_reduce_fusion
  102.9 0.0 copy-start.1
  102.9 4.1 %convert_element_type.52 = f32[2,2048,256]{2,1,0:T(8,128)} convert(bf16[2,2048,256]{2,1,0:T(8,128)(2,1)} %get-tuple-element.14) | non-fusion elementwise | flops 1048576 | bytes 6291456 | tf_op jit(solution)/shard_map/convert_element_type | solution.py:541
  107.0 0.0 copy-done.1
  107.0 0.0 copy-start
  107.0 2.3 %convert_element_type.53 = f32[2,2048,256]{2,1,0:T(8,128)} convert(bf16[2,2048,256]{2,1,0:T(8,128)(2,1)S(1)} %copy-done.1) | non-fusion elementwise | flops 1048576 | bytes 6291456 | tf_op jit(solution)/shard_map/convert_element_type | solution.py:542
  109.3 0.0 copy-done
  109.3 0.0 copy-start.3
  109.3 0.0 copy-start.2
  109.3 2.5 %convert_element_type.54 = f32[2,256,2048]{2,1,0:T(8,128)} convert(bf16[2,256,2048]{2,1,0:T(8,128)(2,1)S(1)} %copy-done) | non-fusion elementwise | flops 1048576 | bytes 6291456 | tf_op jit(solution)/shard_map/convert_element_type | solution.py:543
  111.9 0.0 copy-done.3
  111.9 0.7 copy.17
  112.5 0.0 copy-done.2
  112.5 0.7 copy.18
  (2 shorter events, 0.0 us)
Async XLA Ops:
  4.4 97.8 %copy-start.4 = (s32[256,4]{0,1:T(4,128)S(1)}, s32[256,4]{0,1:T(4,128)}, u32[]{:S(2)}) copy-start(s32[256,4]{0,1:T(4,128)} %param.11) | copy-start | bytes 12292
  102.9 4.1 %copy-start.1 = (bf16[2,2048,256]{2,1,0:T(8,128)(2,1)S(1)}, bf16[2,2048,256]{2,1,0:T(8,128)(2,1)}, u32[]{:S(2)}) copy-start(bf16[2,2048,256]{2,1,0:T(8,128)(2,1)} %get-tuple-element.15) | copy-start | bytes 6291460
  107.0 2.3 %copy-start = (bf16[2,256,2048]{2,1,0:T(8,128)(2,1)S(1)}, bf16[2,256,2048]{2,1,0:T(8,128)(2,1)}, u32[]{:S(2)}) copy-start(bf16[2,256,2048]{2,1,0:T(8,128)(2,1)} %get-tuple-element.16) | copy-start | bytes 6291460
  109.3 2.5 %copy-start.3 = (bf16[256,256]{1,0:T(8,128)(2,1)S(1)}, bf16[256,256]{1,0:T(8,128)(2,1)}, u32[]{:S(2)}) copy-start(bf16[256,256]{1,0:T(8,128)(2,1)} %get-tuple-element.26) | copy-start | bytes 393220
  109.3 3.2 %copy-start.2 = (f32[256,128]{1,0:T(8,128)S(1)}, f32[256,128]{1,0:T(8,128)}, u32[]{:S(2)}) copy-start(f32[256,128]{1,0:T(8,128)} %get-tuple-element.31) | copy-start | bytes 393220
